TPU v7x, 256 devices: a whole 4x4x8 slice. The times are simulated.
256 devices in a mesh: sp: 64 (over z, x, core), tp: 4 (over y).
Axes of the slice: x: 4, y: 4, z: 8, core: 2. Of those that a mesh axis runs over, the one named last changes fastest.
Arguments:
- cot_out: bfloat16 [16384, 2048], P('sp', 'tp'), may hold values from -16 to 16
- route_ids: int32 [16384, 2], P('sp'), may hold values from 0 to 63, all different within a row; in each aligned block of 256 rows (0 to 255, 256 to 511, ...) at most 12 rows name the same one
- route_weight: float32 [16384, 2], P('sp'), may hold values from 0.1 to 1
- expert_inputs: bfloat16 [64, 768, 2048], P('sp'), may hold values from -48 to 48
- w_gate: bfloat16 [64, 2048, 1024], P('sp', None, 'tp'), may hold values from -0.125 to 0.125
- w_up: bfloat16 [64, 2048, 1024], P('sp', None, 'tp'), may hold values from -0.125 to 0.125
- w_down: bfloat16 [64, 1024, 2048], P('sp', 'tp'), may hold values from -0.1875 to 0.1875
- w_proj: bfloat16 [2048, 2048], P('tp'), may hold values from -0.125 to 0.125
- conv_out: bfloat16 [16384, 2048], P('sp', 'tp'), may hold values from -6 to 6
- channel_norm_gain: float32 [2048], P('tp'), may hold values from 0.1 to 1.9
- taps: float32 [31, 2048], P(None, 'tp'), may hold values from -1 to 1
- value_pre: bfloat16 [16384, 2048], P('sp', 'tp'), may hold values from -6 to 6
- gate_pre: bfloat16 [16384, 2048], P('sp', 'tp'), may hold values from -6 to 6
Outputs:
- grad_gate_w: bfloat16 [64, 2048, 1024], P('sp', None, 'tp')
- grad_up_w: bfloat16 [64, 2048, 1024], P('sp', None, 'tp')
- grad_down_w: bfloat16 [64, 1024, 2048], P('sp', 'tp')
- grad_proj: float32 [2048, 2048], P(('tp', 'sp'))
- grad_value: bfloat16 [16384, 2048], P('sp', 'tp')
- grad_gate: bfloat16 [16384, 2048], P('sp', 'tp')
Inputs may be any that keep to these rules, and one draw needn't show every extreme that they name: `route_ids`: among the tokens of one index of sp no expert is chosen more than 12 times, a bound that some block reaches; a token's experts differ.
All inputs are finite; a program needn't handle non-finite values.
Results may differ from a plain program's by a relative error of at most 0.012.
Values may be sent and summed in bfloat16 or wider, within the bound.
No kernel may reach another device: no remote copies, remote signals or barrier semaphores. Data moves between devices by JAX's collectives and lax.ppermute only.
A program may use at most 128 MiB of HBM per device.

v0:
```python
import jax
import jax.numpy as jnp
from jax import lax
from jax.experimental import pallas as pl
from jax.experimental.pallas import tpu as pltpu
from jax.sharding import Mesh
from jax.sharding import PartitionSpec as P

SP = ("sp_0", "sp_1", "sp_2")
PLANE = "sp_0"
COLUMN = "sp_1"
CORE = "sp_2"
TP = "tp"
TP_SP = ("tp", "sp_0", "sp_1", "sp_2")

clamp_limit = 7.0
swish_alpha = 1.702
norm_epsilon = 1e-05
LANES = 128
bf16 = jnp.bfloat16
f32 = jnp.float32


def shifted(value, axis, steps):
    count = lax.axis_size(axis)
    return lax.ppermute(value, axis, [(i, (i + steps) % count) for i in range(count)])


def passed_along(value, axis, steps):
    count = lax.axis_size(axis)
    leading, last = (max(0, -steps), min(count, count - steps))
    return lax.ppermute(value, axis, [(source, source + steps) for source in range(leading, last)])


def dot(a, b, ca, cb):
    return lax.dot_general(a, b, (((ca,), (cb,)), ((), ())), preferred_element_type=f32)


def kernel(body, outs, *args, flops, scratch=(), smem=0, limit=24, staged=range(99), to_hbm=()):
    spaces = [pltpu.SMEM] * smem + [pltpu.VMEM] * (len(args) - smem)
    moved = sum(a.size * a.dtype.itemsize for a in (*args[smem:], *outs))
    args = args[:smem] + tuple(
        pltpu.with_memory_space_constraint(a, pltpu.VMEM if i in staged else pltpu.HBM)
        for i, a in enumerate(args[smem:])
    )
    return pl.pallas_call(
        body,
        out_shape=tuple(
            (pltpu.HBM if i in to_hbm else pltpu.VMEM)(o.shape, o.dtype) for i, o in enumerate(outs)
        ),
        in_specs=[pl.BlockSpec(memory_space=s) for s in spaces],
        out_specs=tuple(pl.BlockSpec(memory_space=pltpu.VMEM) for _ in outs),
        scratch_shapes=list(scratch),
        cost_estimate=pl.CostEstimate(flops=flops, transcendentals=0, bytes_accessed=moved),
        compiler_params=pltpu.CompilerParams(vmem_limit_bytes=limit << 20),
    )(*args)


def struct(shape, dtype=bf16):
    return jax.ShapeDtypeStruct(shape, dtype)


def to_chunks(rows, scratch):
    n, parts = rows.shape[0], rows.shape[1] // LANES
    for j in range(parts):
        scratch[pl.ds(j, n, stride=parts), :] = rows[:, j * LANES : (j + 1) * LANES]


def from_chunks(chunks, scratch, n, parts):
    scratch[...] = chunks.astype(f32)
    pieces = [scratch[pl.ds(j, n, stride=parts), :].astype(bf16) for j in range(parts)]
    return jnp.concatenate(pieces, axis=1)


def dispatch_body(experts, capacity):
    def body(ids_ref, weight_ref, cot_ref, out_ref, dest_ref, scratch):
        tokens = ids_ref.shape[1]
        slots = experts * capacity
        id0, id1 = ids_ref[0:1, :], ids_ref[1:2, :]
        expert = lax.broadcasted_iota(jnp.int32, (LANES, tokens), 0)
        hot0 = (id0 == expert).astype(f32)
        hot1 = (id1 == expert).astype(f32)
        row = lax.broadcasted_iota(jnp.int32, (tokens, tokens), 0)
        col = lax.broadcasted_iota(jnp.int32, (tokens, tokens), 1)
        before = dot((hot0 + hot1).astype(bf16), (row < col).astype(f32).astype(bf16), 1, 0)
        slot0 = jnp.sum(before * hot0, axis=0, keepdims=True).astype(jnp.int32)
        slot1 = jnp.sum(before * hot1, axis=0, keepdims=True).astype(jnp.int32)
        dest0 = id0 * capacity + slot0
        dest1 = id1 * capacity + slot1
        dest_ref[0:1, :] = dest0
        dest_ref[1:2, :] = dest1
        place = lax.broadcasted_iota(jnp.int32, (slots, tokens), 0)
        spread = jnp.where(place == dest0, weight_ref[0:1, :], 0.0) + jnp.where(
            place == dest1, weight_ref[1:2, :], 0.0
        )
        high = spread.astype(bf16)
        low = (spread - high.astype(f32)).astype(bf16)
        cot = cot_ref[...]
        to_chunks(dot(high, cot, 1, 0) + dot(low, cot, 1, 0), scratch)
        out_ref[...] = scratch[...].astype(bf16)

    return body


def pick_body(dest_ref, pick_ref):
    tokens, slots = pick_ref.shape
    row = lax.broadcasted_iota(jnp.int32, (tokens, tokens), 0)
    col = lax.broadcasted_iota(jnp.int32, (tokens, tokens), 1)
    dest0, dest1 = (
        jnp.sum(jnp.where(row == col, dest_ref[k : k + 1, :].astype(f32), 0.0), axis=1, keepdims=True)
        .astype(jnp.int32)
        for k in range(2)
    )
    place = lax.broadcasted_iota(jnp.int32, (tokens, slots), 1)
    pick_ref[...] = ((place == dest0) | (place == dest1)).astype(f32).astype(bf16)


def factors_body(rows_ref, gate_ref, up_ref, act_ref, for_up_ref, for_gate_ref):
    block = rows_ref.shape[0] // 3

    def step(i, _):
        at = pl.ds(pl.multiple_of(i * block, block), block)
        rows = rows_ref[at, :]
        gate_lin = dot(rows, gate_ref[...], 1, 0)
        up_lin = dot(rows, up_ref[...], 1, 0)
        gate_c = jnp.minimum(gate_lin, clamp_limit)
        up_c = jnp.clip(up_lin, -clamp_limit, clamp_limit)
        sigma = jax.nn.sigmoid(swish_alpha * gate_c)
        swish = gate_c * sigma
        act_ref[at, :] = ((up_c + 1.0) * swish).astype(bf16)
        up_open = (up_lin > -clamp_limit) & (up_lin < clamp_limit)
        for_up_ref[at, :] = jnp.where(up_open, swish, 0.0).astype(bf16)
        slope = (up_c + 1.0) * (sigma + swish_alpha * swish * (1.0 - sigma))
        for_gate_ref[at, :] = jnp.where(gate_lin < clamp_limit, slope, 0.0).astype(bf16)
        return 0

    lax.fori_loop(0, 3, step, 0)


def partial_far_body(chunks_ref, far_ref, rows_ref, far_top, far_bot, scratch):
    n, width = rows_ref.shape
    half = n // 2
    rows = from_chunks(chunks_ref[...], scratch, n, width // LANES)
    rows_ref[...] = rows
    value = dot(rows, far_ref[...], 1, 1).astype(bf16)
    far_top[...] = value[:half]
    far_bot[...] = value[half:]


def partial_rest_body(rows_ref, next_ref, prev_ref, own_ref, *outs):
    next_top, next_bot, prev_top, prev_bot, own_out, rows_out = outs
    rows = rows_ref[...]
    half = rows.shape[0] // 2
    rows_out[...] = rows
    for weight, top, bot in ((next_ref, next_top, next_bot), (prev_ref, prev_top, prev_bot)):
        value = dot(rows, weight[...], 1, 1).astype(bf16)
        top[...] = value[:half]
        bot[...] = value[half:]
    own_out[...] = dot(rows, own_ref[...], 1, 1).astype(bf16)


def block_of(ref, index, size):
    return ref[pl.ds(pl.multiple_of(index * size, size), size), :]


def hidden_grad_body(
    at_ref, own_ref, prev_top, near_top, next_bot, near_bot, up_ref, gate_ref, wg_ref, wu_ref,
    d_gate_ref, d_up_ref, far_top, far_bot,
):
    half = prev_top.shape[0]
    size = far_top.shape[1]
    count = wg_ref.shape[0] // size
    own = own_ref[...].astype(f32)
    top = own[:half] + prev_top[...].astype(f32) + near_top[...].astype(f32)
    bot = own[half:] + next_bot[...].astype(f32) + near_bot[...].astype(f32)
    d_act = jnp.concatenate([top, bot], axis=0)
    d_gate = (d_act * gate_ref[...].astype(f32)).astype(bf16)
    d_up = (d_act * up_ref[...].astype(f32)).astype(bf16)
    d_gate_ref[...] = d_gate
    d_up_ref[...] = d_up
    far = lax.rem(at_ref[0] + 2, count)
    value = dot(d_gate, block_of(wg_ref, far, size), 1, 1) + dot(d_up, block_of(wu_ref, far, size), 1, 1)
    value = value.astype(bf16)
    far_top[...] = value[:half]
    far_bot[...] = value[half:]


def input_grad_body(
    at_ref, d_gate_ref, d_up_ref, wg_ref, wu_ref, next_top, next_bot, prev_top, prev_bot, own_out
):
    half = next_top.shape[0]
    size = own_out.shape[1]
    count = wg_ref.shape[0] // size
    d_gate, d_up = d_gate_ref[...], d_up_ref[...]

    def part(shift):
        at = lax.rem(at_ref[0] + shift, count)
        value = dot(d_gate, block_of(wg_ref, at, size), 1, 1)
        value = value + dot(d_up, block_of(wu_ref, at, size), 1, 1)
        return value.astype(bf16)

    value = part(1)
    next_bot[...] = value[half:]
    next_top[...] = value[:half]
    value = part(count - 1)
    prev_top[...] = value[:half]
    prev_bot[...] = value[half:]
    own_out[...] = part(0)


def total_body(own_ref, prev_top, near_top, next_bot, near_bot, out_ref, scratch):
    half = prev_top.shape[0]
    own = own_ref[...].astype(f32)
    top = own[:half] + prev_top[...].astype(f32) + near_top[...].astype(f32)
    bot = own[half:] + next_bot[...].astype(f32) + near_bot[...].astype(f32)
    to_chunks(jnp.concatenate([top, bot], axis=0), scratch)
    out_ref[...] = scratch[...].astype(bf16)


def combine_body(chunks_ref, pick_ref, cot_ref, mix_ref, scratch):
    slots = pick_ref.shape[1]
    rows = from_chunks(chunks_ref[...], scratch, slots, cot_ref.shape[1] // LANES)
    mix = (cot_ref[...].astype(f32) + dot(pick_ref[...], rows, 1, 0)).astype(bf16)
    mix_ref[...] = mix


def down_near_body(at_ref, act_ref, *refs):
    *rows, out_ref = refs
    size = rows[0].shape[1]
    count = out_ref.shape[1] // size
    act = act_ref[...]
    for rows_ref, shift in zip(rows, (0, 1, count - 1)):
        at = lax.rem(at_ref[0] + shift, count)
        value = dot(act, rows_ref[...], 0, 0)
        out_ref[:, pl.ds(pl.multiple_of(at * size, size), size)] = value.astype(bf16)


def down_far_body(at_ref, act_ref, rows_ref, near_ref, *refs):
    *operands, out_ref, one, two, three, block, sem = refs
    for operand, copy in zip(operands, (one, two, three)):
        copy[...] = operand[...]
    size = rows_ref.shape[1]
    block[...] = dot(act_ref[...], rows_ref[...], 0, 0).astype(bf16)
    at = lax.rem(at_ref[0] + 2, out_ref.shape[1] // size)
    put = pltpu.make_async_copy(
        block, out_ref.at[:, pl.ds(pl.multiple_of(at * size, size), size)], sem
    )
    put.start()
    put.wait()


def proj_grad_body(columns):
    def body(core_ref, act_ref, *refs):
        *mixes, send_ref, keep_ref = refs
        size = mixes[0].shape[1]
        rows = act_ref.shape[1] // 2
        block = rows // columns
        first = core_ref[0] == 0
        act = act_ref[...]
        for s, mix_ref in enumerate(mixes):
            value = dot(act, mix_ref[...], 0, 0).reshape(block // 8, columns, 2, 8, size)
            for x in range(columns):
                zero, one = (value[:, x, core].reshape(block, size) for core in range(2))
                at = (slice(x * block, (x + 1) * block), slice(s * size, (s + 1) * size))
                send_ref[at] = jnp.where(first, one, zero).astype(bf16)
                keep_ref[at] = jnp.where(first, zero, one).astype(bf16)

    return body


def pair_sum_body(at_ref, near_ref, near_in_ref, far_ref, far_in_ref, *outs):
    size = outs[0].shape[0]
    count = near_ref.shape[0] // size
    near = near_ref.shape[1]
    for out_ref, shift in zip(outs, (0, 1, count - 1, 2)):
        at = lax.rem(at_ref[0] + shift, count)

        def total(one_ref, two_ref):
            one, two = block_of(one_ref, at, size), block_of(two_ref, at, size)
            return (one.astype(f32) + two.astype(f32)).astype(bf16)

        out_ref[:, :near] = total(near_ref, near_in_ref)
        out_ref[:, near:] = total(far_ref, far_in_ref)


def four_sum_body(*refs):
    *terms, out_ref = refs
    out_ref[...] = sum(term[...].astype(f32) for term in terms).astype(bf16)


def proj_total_body(at_ref, terms_ref, out_ref):
    rows, width = out_ref.shape
    count = 4
    terms = terms_ref[...].astype(f32)
    total = jnp.sum(terms.reshape(terms.shape[0] // rows, rows, width), axis=0)
    size = width // count
    for s, shift in enumerate((0, 1, count - 1, 2)):
        at = lax.rem(at_ref[0] + shift, count)
        out_ref[:, pl.ds(pl.multiple_of(at * size, size), size)] = total[:, s * size : (s + 1) * size]


def split(value, pieces):
    terms = []
    for _ in range(pieces):
        terms.append(value.astype(bf16))
        value = value - terms[-1].astype(f32)
    return terms


def row_sums(first, second, out_ref):
    ones = jnp.ones((8, first.shape[1]), bf16)
    one = sum(dot(ones, term, 1, 1) for term in split(first, 3))
    two = sum(dot(ones, term, 1, 1) for term in split(second, 3))
    row = lax.broadcasted_iota(jnp.int32, out_ref.shape, 0)
    out_ref[...] = jnp.where(row == 0, one, jnp.where(row == 1, two, 0.0))


def along_rows(sums, index):
    row = lax.broadcasted_iota(jnp.int32, (8, LANES), 0)
    chosen = (row == index).astype(f32).astype(bf16)
    return sum(dot(term, chosen, 0, 0) for term in split(sums, 3))


def widened(value, lanes):
    return jnp.concatenate([value] * (lanes // LANES), axis=1)


def stats_body(conv_ref, out_ref):
    conv = conv_ref[...].astype(f32)
    row_sums(conv, conv * conv, out_ref)


def norm_body(channels):
    def body(own, one, two, three, conv_ref, gain_ref, *outs):
        sums = own[...] + one[...] + two[...] + three[...]
        width = conv_ref.shape[1]
        mean = along_rows(sums, 0) / channels
        var = along_rows(sums, 1) / channels - mean * mean
        rstd = lax.rsqrt(var + norm_epsilon)
        xhat = (conv_ref[...].astype(f32) - widened(mean, width)) * widened(rstd, width)
        gain = gain_ref[...]
        normed = xhat * gain
        sigma = jax.nn.sigmoid(normed)
        act_ref, xhat_ref, slope_ref, rstd_ref = outs
        act_ref[...] = (normed * sigma).astype(bf16)
        rstd_ref[...] = rstd
        xhat_ref[...] = xhat
        slope_ref[...] = sigma * (1.0 + normed * (1.0 - sigma)) * gain

    return body


def norm_grad_body(at_ref, own, following, previous, far, proj_ref, xhat_ref, slope_ref, dxh_ref, sums_ref):
    size = own.shape[1]
    count = proj_ref.shape[1] // size
    value = None
    for shift, mix_ref in ((0, own), (1, following), (count - 1, previous), (2, far)):
        at = lax.rem(at_ref[0] + shift, count)
        weight = proj_ref[:, pl.ds(pl.multiple_of(at * size, size), size)]
        term = dot(mix_ref[...], weight, 1, 1)
        value = term if value is None else value + term
    dxh = value * slope_ref[...]
    dxh_ref[...] = dxh
    row_sums(dxh, dxh * xhat_ref[...], sums_ref)


def conv_grad_body(channels):
    def body(own, one, two, three, dxh_ref, xhat_ref, rstd_ref, out_ref, edge_ref):
        sums = own[...] + one[...] + two[...] + three[...]
        width = dxh_ref.shape[1]
        first = widened(along_rows(sums, 0) / channels, width)
        second = widened(along_rows(sums, 1) / channels, width)
        value = widened(rstd_ref[...], width) * (dxh_ref[...] - first - xhat_ref[...] * second)
        out_ref[...] = value
        edge_ref[...] = value[: edge_ref.shape[0]]

    return body


def conv_body(grad_ref, edge_ref, taps_ref, value_ref, gate_ref, value_out, gate_out, extended, moved):
    tokens, width = grad_ref.shape
    reach = taps_ref.shape[0]
    extended[:tokens, :] = grad_ref[...]
    extended[tokens:, :] = edge_ref[...]
    rows = moved.shape[1]
    block = 64

    def step(i, _):
        lanes = pl.ds(pl.multiple_of(i * LANES, LANES), LANES)
        for r in range(8):
            moved[r] = extended[r : r + rows, lanes]
        for start in range(0, tokens, block):
            total = jnp.zeros((block, LANES), f32)
            for offset in range(reach):
                tap = taps_ref[reach - 1 - offset : reach - offset, lanes]
                begin = start + offset // 8 * 8
                total = total + tap * moved[offset % 8, begin : begin + block, :]
            at = slice(start, start + block)
            sigma = jax.nn.sigmoid(gate_ref[at, lanes].astype(f32))
            scaled = total * sigma
            value_out[at, lanes] = scaled.astype(bf16)
            gate = scaled * value_ref[at, lanes].astype(f32) * (1.0 - sigma)
            gate_out[at, lanes] = gate.astype(bf16)
        return 0

    lax.fori_loop(0, width // LANES, step, 0)


def weight_grad_body(rows_ref, gate_ref, up_ref, gate_out, up_out):
    size = gate_ref.shape[1]
    both = jnp.concatenate([gate_ref[...], up_ref[...]], axis=1)

    def step(i, _):
        at = pl.ds(pl.multiple_of(i * size, size), size)
        value = dot(rows_ref[:, at], both, 0, 0)
        gate_out[at, :] = value[:, :size].astype(bf16)
        up_out[at, :] = value[:, size:].astype(bf16)
        return 0

    lax.fori_loop(0, rows_ref.shape[1] // size, step, 0)


def near_body(one_ref, two_ref, out_ref):
    out_ref[...] = (one_ref[...].astype(f32) + two_ref[...].astype(f32)).astype(bf16)


def near_sum(one, two):
    (value,) = kernel(near_body, (struct(one.shape),), one, two, flops=one.size, limit=4)
    return value


def exchanged(value):
    return shifted(value, TP, 1), shifted(value, TP, -1), shifted(value, TP, 2)


def reduce_over_ring(far_top, far_bot, rest):
    far_top_in = shifted(far_top, TP, 1)
    far_bot_in = shifted(far_bot, TP, -1)
    next_top, next_bot, prev_top, prev_bot, own = rest
    next_bot_in = shifted(next_bot, TP, 1)
    prev_top_in = shifted(prev_top, TP, -1)
    near_top = near_sum(next_top, far_top_in)
    near_bot = near_sum(prev_bot, far_bot_in)
    near_top_in = shifted(near_top, TP, 1)
    near_bot_in = shifted(near_bot, TP, -1)
    return own, prev_top_in, near_top_in, next_bot_in, near_bot_in


def per_device(
    cot_out,
    route_ids,
    route_weight,
    expert_inputs,
    w_gate,
    w_up,
    w_down,
    w_proj,
    conv_out,
    channel_norm_gain,
    taps,
    value_pre,
    gate_pre,
):
    experts = lax.axis_size(SP)
    ways = lax.axis_size(TP)
    tok_rows = cot_out.shape[0]
    slot_rows = expert_inputs.shape[1]
    capacity = slot_rows // experts
    local_cols = cot_out.shape[1]
    hidden = w_down.shape[1]
    half = slot_rows // 2
    parts = local_cols // LANES
    chunk_rows = slot_rows * parts
    at = lax.axis_index(TP)
    at_ref = at.reshape(1).astype(jnp.int32)
    core_ref = lax.axis_index(CORE).reshape(1).astype(jnp.int32)
    rows_in, gate_weight, up_weight, down_weight = expert_inputs[0], w_gate[0], w_up[0], w_down[0]
    chunk_scratch = pltpu.VMEM((chunk_rows, LANES), f32)

    outgoing, dest = kernel(
        dispatch_body(experts, capacity),
        (struct((chunk_rows, LANES)), struct((2, tok_rows), jnp.int32)),
        route_ids.T, route_weight.T, cot_out,
        flops=4 * tok_rows * slot_rows * local_cols, scratch=(chunk_scratch,),
        staged=(), to_hbm=(1,),
    )
    moved = lax.all_to_all(
        outgoing.reshape(experts, chunk_rows // experts, LANES), SP, 0, 0, tiled=True
    )
    dest, conv_late, down_late, rows_late, gate_late, up_late, _ = lax.optimization_barrier(
        (dest, conv_out, down_weight, rows_in, gate_weight, up_weight, outgoing)
    )

    def down_block(shift):
        start = (at + shift) % ways * local_cols
        return lax.dynamic_slice_in_dim(down_late, start, local_cols, 1)

    down_own = down_block(0)
    down_next = shifted(down_block(ways - 1), TP, -1)
    down_prev = shifted(down_block(1), TP, 1)
    down_far = shifted(down_block(2), TP, 2)
    act, for_up, for_gate = kernel(
        factors_body,
        (struct((slot_rows, hidden)),) * 3,
        rows_late, gate_late, up_late,
        flops=4 * slot_rows * hidden * local_cols * ways, staged=(),
    )
    (pick,) = kernel(
        pick_body, (struct((tok_rows, slot_rows)),), dest, flops=tok_rows * slot_rows * 8
    )
    channel_total = local_cols * ways
    tokens_8 = struct((8, tok_rows), f32)
    block = struct((tok_rows, local_cols), f32)
    (stats,) = kernel(stats_body, (tokens_8,), conv_late, flops=48 * tok_rows * local_cols, limit=8)
    stats_in = exchanged(stats)
    gain = channel_norm_gain.reshape(1, local_cols)
    moved, act, for_up, for_gate, pick, stats_in = lax.optimization_barrier(
        (moved, act, for_up, for_gate, pick, stats_in)
    )

    rows_near, far_top, far_bot = kernel(
        partial_far_body,
        (struct((slot_rows, local_cols)),) + (struct((half, hidden)),) * 2,
        moved.reshape(chunk_rows, LANES), down_far,
        flops=2 * slot_rows * local_cols * hidden, scratch=(chunk_scratch,),
    )
    *rest, rows_cot = kernel(
        partial_rest_body,
        (struct((half, hidden)),) * 4
        + (struct((slot_rows, hidden)), struct((slot_rows, local_cols))),
        rows_near, down_next, down_prev, down_own,
        flops=6 * slot_rows * local_cols * hidden, to_hbm=(5,),
    )
    act_terms = reduce_over_ring(far_top, far_bot, rest)
    d_gate, d_up, far_top, far_bot = kernel(
        hidden_grad_body,
        (struct((slot_rows, hidden)),) * 2 + (struct((half, local_cols)),) * 2,
        at_ref, *act_terms, for_up, for_gate, gate_weight, up_weight,
        flops=4 * slot_rows * local_cols * hidden, smem=1,
    )
    rest = kernel(
        input_grad_body,
        (struct((half, local_cols)),) * 4 + (struct((slot_rows, local_cols)),),
        at_ref, d_gate, d_up, gate_weight, up_weight,
        flops=12 * slot_rows * local_cols * hidden, smem=1,
    )
    grad_terms = reduce_over_ring(far_top, far_bot, rest)
    (returning,) = kernel(
        total_body,
        (struct((chunk_rows, LANES)),),
        *grad_terms,
        flops=slot_rows * local_cols * 8, scratch=(chunk_scratch,),
    )
    coming = lax.all_to_all(
        returning.reshape(experts, chunk_rows // experts, LANES), SP, 0, 0, tiled=True
    )
    grad_gate_part, grad_up_part = kernel(
        weight_grad_body,
        (struct((local_cols * ways, hidden)),) * 2,
        rows_in, d_gate, d_up,
        flops=4 * slot_rows * hidden * local_cols * ways, to_hbm=(0, 1),
    )
    rows_cot, _ = lax.optimization_barrier((rows_cot, returning))
    rows_prev = shifted(rows_cot, TP, 1)
    rows_next = shifted(rows_cot, TP, -1)
    coming, grad_gate_part, grad_up_part = lax.optimization_barrier(
        (coming, grad_gate_part, grad_up_part)
    )
    (mix,) = kernel(
        combine_body,
        (struct((tok_rows, local_cols)),),
        coming.reshape(chunk_rows, LANES), pick, cot_out,
        flops=2 * tok_rows * slot_rows * local_cols, scratch=(chunk_scratch,),
    )
    mix_far = shifted(mix, TP, 2)
    mix_prev = shifted(mix, TP, 1)
    mix_next = shifted(mix, TP, -1)
    conv_mid, _ = lax.optimization_barrier((conv_out, mix))
    act_conv, xhat, slope, rstd = kernel(
        norm_body(channel_total),
        (struct((tok_rows, local_cols)), block, block, struct((tok_rows, LANES), f32)),
        stats, *stats_in, conv_mid, gain,
        flops=20 * tok_rows * local_cols, limit=8, staged=(),
    )
    columns, planes = lax.axis_size(COLUMN), lax.axis_size(PLANE)
    width = local_cols * ways
    core_rows = local_cols // 2
    column_rows = core_rows // columns

    def proj_terms(mixes):
        return kernel(
            proj_grad_body(columns),
            (struct((core_rows, local_cols * len(mixes))),) * 2,
            core_ref, act_conv, *mixes,
            flops=2 * len(mixes) * tok_rows * local_cols * local_cols, smem=1,
            to_hbm=(1,),
        )

    send, keep = proj_terms((mix, mix_next, mix_prev))
    came = shifted(send, CORE, 1)
    send_far, keep_far = proj_terms((mix_far,))
    came_far = shifted(send_far, CORE, 1)
    pair_own, pair_next, pair_prev, pair_far = kernel(
        pair_sum_body,
        (struct((column_rows, width)),) * 4,
        lax.axis_index(COLUMN).reshape(1).astype(jnp.int32), keep, came, keep_far, came_far,
        flops=core_rows * width, smem=1, limit=8, staged=(1, 3),
    )
    far_pair = shifted(pair_far, COLUMN, 2)
    near_pairs = (shifted(pair_next, COLUMN, 1), shifted(pair_prev, COLUMN, -1))
    (column_sum,) = kernel(
        four_sum_body,
        (struct((column_rows, width)),),
        pair_own, far_pair, *near_pairs,
        flops=column_rows * width * 4, limit=8,
    )
    terms = lax.all_to_all(
        column_sum.reshape(planes, column_rows // planes, width), PLANE, 0, 0, tiled=True
    )
    (grad_proj,) = kernel(
        proj_total_body,
        (struct((column_rows // planes, width), f32),),
        at_ref, terms.reshape(column_rows, width),
        flops=column_rows * width, smem=1, limit=8, to_hbm=(0,),
    )
    dxh, sums = kernel(
        norm_grad_body,
        (block, tokens_8),
        at_ref, mix, mix_next, mix_prev, mix_far, w_proj, xhat, slope,
        flops=2 * tok_rows * local_cols * local_cols * ways, smem=1,
        staged=(0, 1, 2, 3, 5, 6),
    )
    sums_in = exchanged(sums)
    rows_far = shifted(rows_cot, TP, 2)
    (grad_down,) = kernel(
        down_near_body,
        (struct((hidden, width)),),
        at_ref, act, rows_cot, rows_next, rows_prev,
        flops=6 * slot_rows * hidden * local_cols, smem=1, to_hbm=(0,), staged=(),
    )
    hbm = pl.BlockSpec(memory_space=pltpu.HBM)
    vmem = pl.BlockSpec(memory_space=pltpu.VMEM)
    conv_operands = (taps, value_pre, gate_pre)
    grad_down, *conv_operands = pl.pallas_call(
        down_far_body,
        out_shape=(struct((hidden, width)),)
        + tuple(pltpu.VMEM(v.shape, v.dtype) for v in conv_operands),
        in_specs=[pl.BlockSpec(memory_space=pltpu.SMEM), vmem, vmem, hbm, vmem, vmem, vmem],
        out_specs=(hbm, vmem, vmem, vmem),
        scratch_shapes=[pltpu.VMEM((hidden, local_cols), bf16), pltpu.SemaphoreType.DMA],
        input_output_aliases={3: 0},
        cost_estimate=pl.CostEstimate(
            flops=2 * slot_rows * hidden * local_cols, transcendentals=0, bytes_accessed=1 << 20
        ),
        compiler_params=pltpu.CompilerParams(vmem_limit_bytes=24 << 20),
        name="down_far",
    )(
        at_ref,
        *(pltpu.with_memory_space_constraint(v, pltpu.HBM) for v in (act, rows_far, grad_down, *conv_operands)),
    )
    reach = taps.shape[0]
    convolution_gradient, edge = kernel(
        conv_grad_body(channel_total),
        (block, struct((32, local_cols), f32)),
        sums, *sums_in, dxh, xhat, rstd,
        flops=8 * tok_rows * local_cols, limit=8,
    )
    following = passed_along(edge, SP, -1)
    following, grad_down = lax.optimization_barrier((following, grad_down))
    grad_value, grad_gate = kernel(
        conv_body,
        (struct((tok_rows, local_cols)),) * 2,
        convolution_gradient, following, *conv_operands,
        flops=2 * reach * tok_rows * local_cols, limit=8, to_hbm=(0, 1),
        scratch=(
            pltpu.VMEM((tok_rows + edge.shape[0], local_cols), f32),
            pltpu.VMEM((8, tok_rows + 24, LANES), f32),
        ),
    )
    return (
        grad_gate_part[None],
        grad_up_part[None],
        grad_down[None],
        grad_proj,
        grad_value,
        grad_gate,
    )


def solution(mesh):
    finer = Mesh(mesh.devices.reshape(8, 4, 2, mesh.shape["tp"]), ("sp_0", "sp_1", "sp_2", "tp"))
    placed = (
        P(SP, "tp"),
        P(SP, None),
        P(SP, None),
        P(SP, None, None),
        P(SP, None, "tp"),
        P(SP, None, "tp"),
        P(SP, "tp", None),
        P("tp", None),
        P(SP, "tp"),
        P("tp"),
        P(None, "tp"),
        P(SP, "tp"),
        P(SP, "tp"),
    )

    return jax.shard_map(
        per_device,
        mesh=finer,
        in_specs=placed,
        out_specs=(
            P(SP, None, "tp"),
            P(SP, None, "tp"),
            P(SP, "tp", None),
            P(TP_SP, None),
            P(SP, "tp"),
            P(SP, "tp"),
        ),
        check_vma=False,
    )
```

profile of v0, /device:TPU:1, one launch (start us, length us, event | category | flops | bytes accessed | tf_op | source)
XLA Modules:
  0.0 203.7 jit_solution(1254433260217154630)
XLA Ops:
  0.7 2.8 %shard_map.172 = (bf16[3072,128]{1,0:T(8,128)(2,1)}, s32[2,256]{1,0:T(2,128)}) custom-call(s32[2,256]{1,0:T(2,128)} %bitcast.33, f32[2,256]{1,0:T(2,128)} %bitcast.34, bf16[256,512]{1,0:T(8,128)(2,1)} %cot_ref.3), custom_call_target="tpu_custom_call" | custom-call | flops 402653184 | bytes 1054720 | tf_op jit(solution)/shard_map/pallas_call | solution.py:46
  3.5 13.0 %all-to-all-start = ((bf16[64,48,128]{2,1,0:T(8,128)(2,1)}), bf16[64,48,128]{2,1,0:T(8,128)(2,1)S(1)}, u32[]{:S(2)}, u32[]{:S(2)}) async-start(bf16[64,48,128]{2,1,0:T(8,128)(2,1)} %bitcast.3), calls=%async_computation | async-start | bytes 1572864 | tf_op jit(solution)/shard_map/all_to_all | solution.py:487
  17.5 2.9 %collective-permute-start.3 = (bf16[256,512]{1,0:T(8,128)(2,1)}, bf16[256,512]{1,0:T(8,128)(2,1)}, u32[]{:S(2)}, u32[]{:S(2)}) collective-permute-start(bf16[256,512]{1,0:T(8,128)(2,1)} %get-tuple-element.145), channel_id=1, source_target_pairs={{0,2},{1,3},{2,0},{3,1},{4,6},{5,7},{6,4},{7,5},{8,10},{9,11},{10,... | collective-permute-start | bytes 786440 | tf_op jit(solution)/shard_map/ppermute | solution.py:26
  21.3 2.3 %collective-permute-start.1 = (f32[8,256]{1,0:T(8,128)S(1)}, f32[8,256]{1,0:T(8,128)S(1)}, u32[]{:S(2)}, u32[]{:S(2)}) collective-permute-start(f32[8,256]{1,0:T(8,128)S(1)} %shard_map.175.own), channel_id=1, source_target_pairs={{0,3},{1,0},{2,1},{3,2},{4,7},{5,4},{6,5},{7,6},{8,11},{9,8},{10,9... | collective-permute-start | bytes 24584 | tf_op jit(solution)/shard_map/ppermute | solution.py:26
  26.0 2.3 %collective-permute-start.5 = (bf16[256,512]{1,0:T(8,128)(2,1)}, bf16[256,512]{1,0:T(8,128)(2,1)}, u32[]{:S(2)}, u32[]{:S(2)}) collective-permute-start(bf16[256,512]{1,0:T(8,128)(2,1)} %get-tuple-element.143), channel_id=1, source_target_pairs={{0,1},{1,2},{2,3},{3,0},{4,5},{5,6},{6,7},{7,4},{8,9},{9,10},{10,1... | collective-permute-start | bytes 786440 | tf_op jit(solution)/shard_map/ppermute | solution.py:26
  28.3 5.0 %shard_map.173 = (bf16[768,256]{1,0:T(8,128)(2,1)S(1)}, bf16[768,256]{1,0:T(8,128)(2,1)S(1)}, bf16[768,256]{1,0:T(8,128)(2,1)S(1)}) custom-call(bf16[768,2048]{1,0:T(8,128)(2,1)} %bitcast.28, bf16[2048,256]{1,0:T(8,128)(2,1)} %bitcast.22, bf16[2048,256]{1,0:T(8,128)(2,1)} %bitcast.25), custom_call_target="tpu_custom_call" | custom-call | flops 1610612736 | bytes 6422528 | tf_op jit(solution)/shard_map/pallas_call | solution.py:46
  35.5 4.0 %all-to-all-done = bf16[64,48,128]{2,1,0:T(8,128)(2,1)S(1)} async-done(((bf16[64,48,128]{2,1,0:T(8,128)(2,1)}), bf16[64,48,128]{2,1,0:T(8,128)(2,1)S(1)}, u32[]{:S(2)}, u32[]{:S(2)}) %all-to-all-start) | async-done | bytes 786464 | tf_op jit(solution)/shard_map/all_to_all | solution.py:487
  41.0 2.8 %collective-permute-start.10 = (bf16[384,256]{1,0:T(8,128)(2,1)S(1)}, bf16[384,256]{1,0:T(8,128)(2,1)S(1)}, u32[]{:S(2)}, u32[]{:S(2)}) collective-permute-start(bf16[384,256]{1,0:T(8,128)(2,1)S(1)} %get-tuple-element.93), channel_id=1, source_target_pairs={{0,3},{1,0},{2,1},{3,2},{4,7},{5,4},{6,5},{7,6},{8,11},{9,8},{10,9... | collective-permute-start | bytes 589832 | tf_op jit(solution)/shard_map/ppermute | solution.py:26
  43.9 2.4 %shard_map.177 = (bf16[384,256]{1,0:T(8,128)(2,1)S(1)}, bf16[384,256]{1,0:T(8,128)(2,1)S(1)}, bf16[384,256]{1,0:T(8,128)(2,1)S(1)}, bf16[384,256]{1,0:T(8,128)(2...) custom-call(bf16[768,512]{1,0:T(8,128)(2,1)S(1)} %get-tuple-element.86.rows_ref, ...), custom_call_target="tpu_custom_call" | custom-call | flops 603979776 | bytes 3538944 | tf_op jit(solution)/shard_map/pallas_call | solution.py:46
  46.2 2.7 %collective-permute-start.6 = (bf16[384,256]{1,0:T(8,128)(2,1)S(1)}, bf16[384,256]{1,0:T(8,128)(2,1)S(1)}, u32[]{:S(2)}, u32[]{:S(2)}) collective-permute-start(bf16[384,256]{1,0:T(8,128)(2,1)S(1)} %get-tuple-element.88), channel_id=1, source_target_pairs={{0,3},{1,0},{2,1},{3,2},{4,7},{5,4},{6,5},{7,6},{8,11},{9,8},{10,9... | collective-permute-start | bytes 589832 | tf_op jit(solution)/shard_map/ppermute | solution.py:26
  49.0 2.9 %collective-permute-start.11 = (bf16[384,256]{1,0:T(8,128)(2,1)S(1)}, bf16[384,256]{1,0:T(8,128)(2,1)S(1)}, u32[]{:S(2)}, u32[]{:S(2)}) collective-permute-start(bf16[384,256]{1,0:T(8,128)(2,1)S(1)} %shard_map.179), channel_id=1, source_target_pairs={{0,3},{1,0},{2,1},{3,2},{4,7},{5,4},{6,5},{7,6},{8,11},{9,8},{10,9... | collective-permute-start | bytes 589832 | tf_op jit(solution)/shard_map/ppermute | solution.py:26
  52.1 3.0 %collective-permute-done.9.next_bot = bf16[384,256]{1,0:T(8,128)(2,1)S(1)} collective-permute-done((bf16[384,256]{1,0:T(8,128)(2,1)S(1)}, bf16[384,256]{1,0:T(8,128)(2,1)S(1)}, u32[]{:S(2)}, u32[]{:S(2)}) %collective-permute-start.9) | collective-permute-done | bytes 196640 | tf_op jit(solution)/shard_map/ppermute | solution.py:26
  56.6 3.2 %collective-permute-done.8.near_top = bf16[384,256]{1,0:T(8,128)(2,1)S(1)} collective-permute-done((bf16[384,256]{1,0:T(8,128)(2,1)S(1)}, bf16[384,256]{1,0:T(8,128)(2,1)S(1)}, u32[]{:S(2)}, u32[]{:S(2)}) %collective-permute-start.8) | collective-permute-done | bytes 196640 | tf_op jit(solution)/shard_map/ppermute | solution.py:26
  65.0 4.4 %collective-permute-done.16.two_ref = bf16[384,512]{1,0:T(8,128)(2,1)S(1)} collective-permute-done((bf16[384,512]{1,0:T(8,128)(2,1)S(1)}, bf16[384,512]{1,0:T(8,128)(2,1)S(1)}, u32[]{:S(2)}, u32[]{:S(2)}) %collective-permute-start.16) | collective-permute-done | bytes 393248 | tf_op jit(solution)/shard_map/ppermute | solution.py:26
  71.5 6.3 %collective-permute-done.12.prev_top = bf16[384,512]{1,0:T(8,128)(2,1)S(1)} collective-permute-done((bf16[384,512]{1,0:T(8,128)(2,1)S(1)}, bf16[384,512]{1,0:T(8,128)(2,1)S(1)}, u32[]{:S(2)}, u32[]{:S(2)}) %collective-permute-start.12) | collective-permute-done | bytes 393248 | tf_op jit(solution)/shard_map/ppermute | solution.py:26
  79.2 7.0 %collective-permute-done.17.near_bot = bf16[384,512]{1,0:T(8,128)(2,1)S(1)} collective-permute-done((bf16[384,512]{1,0:T(8,128)(2,1)S(1)}, bf16[384,512]{1,0:T(8,128)(2,1)S(1)}, u32[]{:S(2)}, u32[]{:S(2)}) %collective-permute-start.17) | collective-permute-done | bytes 393248 | tf_op jit(solution)/shard_map/ppermute | solution.py:26
  89.0 7.8 %all-to-all-start.1 = ((bf16[64,48,128]{2,1,0:T(8,128)(2,1)}), bf16[64,48,128]{2,1,0:T(8,128)(2,1)S(1)}, u32[]{:S(2)}, u32[]{:S(2)}) async-start(bf16[64,48,128]{2,1,0:T(8,128)(2,1)} %bitcast.9), calls=%async_computation.1 | async-start | bytes 1572864 | tf_op jit(solution)/shard_map/all_to_all | solution.py:554
  98.7 4.7 %shard_map.185 = (bf16[2048,256]{1,0:T(8,128)(2,1)}, bf16[2048,256]{1,0:T(8,128)(2,1)}) custom-call(bf16[768,2048]{1,0:T(8,128)(2,1)S(1)} %bitcast.29, bf16[768,256]{1,0:T(8,128)(2,1)S(1)} %copy-done.13, bf16[768,256]{1,0:T(8,128)(2,1)S(1)} %copy-done.15), custom_call_target="tpu_custom_call" | custom-call | flops 1610612736 | bytes 6029312 | tf_op jit(solution)/shard_map/pallas_call | solution.py:46
  103.4 16.4 %all-to-all-done.1 = bf16[64,48,128]{2,1,0:T(8,128)(2,1)S(1)} async-done(((bf16[64,48,128]{2,1,0:T(8,128)(2,1)}), bf16[64,48,128]{2,1,0:T(8,128)(2,1)S(1)}, u32[]{:S(2)}, u32[]{:S(2)}) %all-to-all-start.1) | async-done | bytes 786464 | tf_op jit(solution)/shard_map/all_to_all | solution.py:554
  123.3 4.2 %collective-permute-done.18.following.refs_1_ = bf16[256,512]{1,0:T(8,128)(2,1)S(1)} collective-permute-done((bf16[256,512]{1,0:T(8,128)(2,1)S(1)}, bf16[256,512]{1,0:T(8,128)(2,1)S(1)}, u32[]{:S(2)}, u32[]{:S(2)}) %collective-permute-start.18) | collective-permute-done | bytes 262176 | tf_op jit(solution)/shard_map/ppermute | solution.py:26
  132.7 8.7 %collective-permute-done.20.far.refs_0_ = bf16[256,512]{1,0:T(8,128)(2,1)S(1)} collective-permute-done((bf16[256,512]{1,0:T(8,128)(2,1)S(1)}, bf16[256,512]{1,0:T(8,128)(2,1)S(1)}, u32[]{:S(2)}, u32[]{:S(2)}) %collective-permute-start.20) | collective-permute-done | bytes 262176 | tf_op jit(solution)/shard_map/ppermute | solution.py:26
  149.8 5.2 %collective-permute-done.30.refs_1_ = bf16[64,2048]{1,0:T(8,128)(2,1)S(1)} collective-permute-done((bf16[64,2048]{1,0:T(8,128)(2,1)S(1)}, bf16[64,2048]{1,0:T(8,128)(2,1)S(1)}, u32[]{:S(2)}, u32[]{:S(2)}) %collective-permute-start.30) | collective-permute-done | bytes 262176 | tf_op jit(solution)/shard_map/ppermute | solution.py:26
  156.0 5.3 %collective-permute-done.31.refs_2_ = bf16[64,2048]{1,0:T(8,128)(2,1)S(1)} collective-permute-done((bf16[64,2048]{1,0:T(8,128)(2,1)S(1)}, bf16[64,2048]{1,0:T(8,128)(2,1)S(1)}, u32[]{:S(2)}, u32[]{:S(2)}) %collective-permute-start.31) | collective-permute-done | bytes 262176 | tf_op jit(solution)/shard_map/ppermute | solution.py:26
  162.1 3.9 %all-to-all-start.2 = ((bf16[8,8,2048]{2,1,0:T(8,128)(2,1)}), bf16[8,8,2048]{2,1,0:T(8,128)(2,1)S(1)}, u32[]{:S(2)}, u32[]{:S(2)}) async-start(bf16[8,8,2048]{2,1,0:T(8,128)(2,1)} %bitcast.17), calls=%async_computation.2 | async-start | bytes 524288 | tf_op jit(solution)/shard_map/all_to_all | solution.py:617
  166.0 2.8 %shard_map.188 = (f32[256,512]{1,0:T(8,128)S(1)}, f32[8,256]{1,0:T(8,128)S(1)}) custom-call(s32[1]{0:T(128)} %bitcast.at_ref, bf16[256,512]{1,0:T(8,128)(2,1)S(1)} %shard_map.186.own.refs_0_, bf16[256,512]{1,0:T(8,128)(2,1)S(1)} %collective-permute-done.18.following.refs_1_, bf16[256,512]{1,0:T(8,128)(2,1)S(1)} %collective-permute-done.19.previous.refs_2_, ...), custom_call_target="tpu_custom_call" | custom-call | flops 536870912 | bytes 4726784 | tf_op jit(solution)/shard_map/pallas_call | solution.py:46
  168.9 2.7 %collective-permute-start.22 = (f32[8,256]{1,0:T(8,128)S(1)}, f32[8,256]{1,0:T(8,128)S(1)}, u32[]{:S(2)}, u32[]{:S(2)}) collective-permute-start(f32[8,256]{1,0:T(8,128)S(1)} %get-tuple-element.117.own), channel_id=1, source_target_pairs={{0,3},{1,0},{2,1},{3,2},{4,7},{5,4},{6,5},{7,6},{8,11},{9,8},{10,9... | collective-permute-start | bytes 24584 | tf_op jit(solution)/shard_map/ppermute | solution.py:26
  171.5 13.8 %collective-permute-done.21.one = f32[8,256]{1,0:T(8,128)S(1)} collective-permute-done((f32[8,256]{1,0:T(8,128)S(1)}, f32[8,256]{1,0:T(8,128)S(1)}, u32[]{:S(2)}, u32[]{:S(2)}) %collective-permute-start.21) | collective-permute-done | bytes 8224 | tf_op jit(solution)/shard_map/ppermute | solution.py:26
  185.3 4.0 %collective-permute-done.23.three = f32[8,256]{1,0:T(8,128)S(1)} collective-permute-done((f32[8,256]{1,0:T(8,128)S(1)}, f32[8,256]{1,0:T(8,128)S(1)}, u32[]{:S(2)}, u32[]{:S(2)}) %collective-permute-start.23) | collective-permute-done | bytes 8224 | tf_op jit(solution)/shard_map/ppermute | solution.py:26
  189.7 3.8 %collective-permute-start.24 = (f32[32,512]{1,0:T(8,128)S(1)}, f32[32,512]{1,0:T(8,128)S(1)}, u32[]{:S(2)}, u32[]{:S(2)}) collective-permute-start(f32[32,512]{1,0:T(8,128)S(1)} %get-tuple-element.120), channel_id=1, source_target_pairs={{4,0},{8,4},{12,8},{16,12},{20,16},{24,20},{28,24},{32,28},{36,32}... | collective-permute-start | bytes 196616 | tf_op jit(solution)/shard_map/ppermute | solution.py:32
  193.5 3.5 %shard_map.190.near_ref = bf16[256,2048]{1,0:T(8,128)(2,1)} custom-call(s32[1]{0:T(128)} %bitcast.at_ref, bf16[768,256]{1,0:T(8,128)(2,1)} %copy-done, bf16[768,512]{1,0:T(8,128)(2,1)} %get-tuple-element.123.refs_0_, bf16[768,512]{1,0:T(8,128)(2,1)} %collective-permute-done.26.refs_1_, bf16[768,512]{1,0:T(8,128)(2,1)} %collective-permute-done.27.refs_2_), custom_call_target="tpu_custom_call" | custom-call | flops 603979776 | bytes 3801088 | tf_op jit(solution)/shard_map/pallas_call | solution.py:46
  198.0 2.5 %down_far.1 = (bf16[256,2048]{1,0:T(8,128)(2,1)}, f32[31,512]{1,0:T(8,128)S(1)}, bf16[256,512]{1,0:T(8,128)(2,1)S(1)}, bf16[256,512]{1,0:T(8,128)(2,1)S(1)}) custom-call(s32[1]{0:T(128)} %bitcast.at_ref, bf16[768,256]{1,0:T(8,128)(2,1)} %copy-done, bf16[768,512]{1,0:T(8,128)(2,1)} %copy-done.17, ...), custom_call_target="tpu_custom_call", output_to_operand_aliasing={{0}: (3, {})} | custom-call | flops 201326592 | bytes 1048576 | tf_op jit(solution)/shard_map/down_far/pallas_call | solution.py:644
  200.6 2.4 %shard_map.196 = (bf16[256,512]{1,0:T(8,128)(2,1)}, bf16[256,512]{1,0:T(8,128)(2,1)}) custom-call(f32[256,512]{1,0:T(8,128)S(1)} %get-tuple-element.135.grad_ref, f32[32,512]{1,0:T(8,128)S(1)} %collective-permute-done.24.edge_ref, f32[31,512]{1,0:T(8,128)S(1)} %get-tuple-element.137.taps_ref, bf16[256,512]{1,0:T(8,128)(2,1)S(1)} %get-tuple-element.138.value_ref, ...), custom_call_target="tpu_custom_call" | custom-call | flops 8126464 | bytes 1701888 | tf_op jit(solution)/shard_map/pallas_call | solution.py:46
  (107 shorter events, 44.0 us)
Async XLA Ops:
  3.5 36.0 %all-to-all-start = ((bf16[64,48,128]{2,1,0:T(8,128)(2,1)}), bf16[64,48,128]{2,1,0:T(8,128)(2,1)S(1)}, u32[]{:S(2)}, u32[]{:S(2)}) async-start(bf16[64,48,128]{2,1,0:T(8,128)(2,1)} %bitcast.3), calls=%async_computation | async-start | bytes 1572864 | tf_op jit(solution)/shard_map/all_to_all | solution.py:487
  17.5 22.0 %collective-permute-start.3 = (bf16[256,512]{1,0:T(8,128)(2,1)}, bf16[256,512]{1,0:T(8,128)(2,1)}, u32[]{:S(2)}, u32[]{:S(2)}) collective-permute-start(bf16[256,512]{1,0:T(8,128)(2,1)} %get-tuple-element.145), channel_id=1, source_target_pairs={{0,2},{1,3},{2,0},{3,1},{4,6},{5,7},{6,4},{7,5},{8,10},{9,11},{10,... | collective-permute-start | bytes 786440 | tf_op jit(solution)/shard_map/ppermute | solution.py:26
  21.3 13.7 %collective-permute-start.1 = (f32[8,256]{1,0:T(8,128)S(1)}, f32[8,256]{1,0:T(8,128)S(1)}, u32[]{:S(2)}, u32[]{:S(2)}) collective-permute-start(f32[8,256]{1,0:T(8,128)S(1)} %shard_map.175.own), channel_id=1, source_target_pairs={{0,3},{1,0},{2,1},{3,2},{4,7},{5,4},{6,5},{7,6},{8,11},{9,8},{10,9... | collective-permute-start | bytes 24584 | tf_op jit(solution)/shard_map/ppermute | solution.py:26
  23.6 11.9 %collective-permute-start.2 = (f32[8,256]{1,0:T(8,128)S(1)}, f32[8,256]{1,0:T(8,128)}, u32[]{:S(2)}, u32[]{:S(2)}) collective-permute-start(f32[8,256]{1,0:T(8,128)S(1)} %shard_map.175.own), channel_id=1, source_target_pairs={{0,2},{1,3},{2,0},{3,1},{4,6},{5,7},{6,4},{7,5},{8,10},{9,11},{10,... | collective-permute-start | bytes 24584 | tf_op jit(solution)/shard_map/ppermute | solution.py:26
  23.6 20.3 %collective-permute-start.4 = (bf16[256,512]{1,0:T(8,128)(2,1)}, bf16[256,512]{1,0:T(8,128)(2,1)}, u32[]{:S(2)}, u32[]{:S(2)}) collective-permute-start(bf16[256,512]{1,0:T(8,128)(2,1)} %get-tuple-element.144), channel_id=1, source_target_pairs={{0,3},{1,0},{2,1},{3,2},{4,7},{5,4},{6,5},{7,6},{8,11},{9,8},{10,9... | collective-permute-start | bytes 786440 | tf_op jit(solution)/shard_map/ppermute | solution.py:26
  26.0 17.9 %collective-permute-start.5 = (bf16[256,512]{1,0:T(8,128)(2,1)}, bf16[256,512]{1,0:T(8,128)(2,1)}, u32[]{:S(2)}, u32[]{:S(2)}) collective-permute-start(bf16[256,512]{1,0:T(8,128)(2,1)} %get-tuple-element.143), channel_id=1, source_target_pairs={{0,1},{1,2},{2,3},{3,0},{4,5},{5,6},{6,7},{7,4},{8,9},{9,10},{10,1... | collective-permute-start | bytes 786440 | tf_op jit(solution)/shard_map/ppermute | solution.py:26
  41.0 7.9 %collective-permute-start.10 = (bf16[384,256]{1,0:T(8,128)(2,1)S(1)}, bf16[384,256]{1,0:T(8,128)(2,1)S(1)}, u32[]{:S(2)}, u32[]{:S(2)}) collective-permute-start(bf16[384,256]{1,0:T(8,128)(2,1)S(1)} %get-tuple-element.93), channel_id=1, source_target_pairs={{0,3},{1,0},{2,1},{3,2},{4,7},{5,4},{6,5},{7,6},{8,11},{9,8},{10,9... | collective-permute-start | bytes 589832 | tf_op jit(solution)/shard_map/ppermute | solution.py:26
  43.8 8.1 %collective-permute-start.7 = (bf16[384,256]{1,0:T(8,128)(2,1)S(1)}, bf16[384,256]{1,0:T(8,128)(2,1)S(1)}, u32[]{:S(2)}, u32[]{:S(2)}) collective-permute-start(bf16[384,256]{1,0:T(8,128)(2,1)S(1)} %get-tuple-element.90), channel_id=1, source_target_pairs={{0,1},{1,2},{2,3},{3,0},{4,5},{5,6},{6,7},{7,4},{8,9},{9,10},{10,1... | collective-permute-start | bytes 589832 | tf_op jit(solution)/shard_map/ppermute | solution.py:26
  48.9 6.1 %collective-permute-start.9 = (bf16[384,256]{1,0:T(8,128)(2,1)S(1)}, bf16[384,256]{1,0:T(8,128)(2,1)S(1)}, u32[]{:S(2)}, u32[]{:S(2)}) collective-permute-start(bf16[384,256]{1,0:T(8,128)(2,1)S(1)} %get-tuple-element.91), channel_id=1, source_target_pairs={{0,1},{1,2},{2,3},{3,0},{4,5},{5,6},{6,7},{7,4},{8,9},{9,10},{10,1... | collective-permute-start | bytes 589832 | tf_op jit(solution)/shard_map/ppermute | solution.py:26
  49.0 7.6 %collective-permute-start.11 = (bf16[384,256]{1,0:T(8,128)(2,1)S(1)}, bf16[384,256]{1,0:T(8,128)(2,1)S(1)}, u32[]{:S(2)}, u32[]{:S(2)}) collective-permute-start(bf16[384,256]{1,0:T(8,128)(2,1)S(1)} %shard_map.179), channel_id=1, source_target_pairs={{0,3},{1,0},{2,1},{3,2},{4,7},{5,4},{6,5},{7,6},{8,11},{9,8},{10,9... | collective-permute-start | bytes 589832 | tf_op jit(solution)/shard_map/ppermute | solution.py:26
  52.0 7.8 %collective-permute-start.8 = (bf16[384,256]{1,0:T(8,128)(2,1)S(1)}, bf16[384,256]{1,0:T(8,128)(2,1)S(1)}, u32[]{:S(2)}, u32[]{:S(2)}) collective-permute-start(bf16[384,256]{1,0:T(8,128)(2,1)S(1)} %shard_map.178), channel_id=1, source_target_pairs={{0,1},{1,2},{2,3},{3,0},{4,5},{5,6},{6,7},{7,4},{8,9},{9,10},{10,1... | collective-permute-start | bytes 589832 | tf_op jit(solution)/shard_map/ppermute | solution.py:26
  60.5 8.9 %collective-permute-start.16 = (bf16[384,512]{1,0:T(8,128)(2,1)S(1)}, bf16[384,512]{1,0:T(8,128)(2,1)S(1)}, u32[]{:S(2)}, u32[]{:S(2)}) collective-permute-start(bf16[384,512]{1,0:T(8,128)(2,1)S(1)} %get-tuple-element.104), channel_id=1, source_target_pairs={{0,3},{1,0},{2,1},{3,2},{4,7},{5,4},{6,5},{7,6},{8,11},{9,8},{10,9... | collective-permute-start | bytes 1179656 | tf_op jit(solution)/shard_map/ppermute | solution.py:26
  60.8 10.5 %collective-permute-start.13 = (bf16[384,512]{1,0:T(8,128)(2,1)S(1)}, bf16[384,512]{1,0:T(8,128)(2,1)S(1)}, u32[]{:S(2)}, u32[]{:S(2)}) collective-permute-start(bf16[384,512]{1,0:T(8,128)(2,1)S(1)} %get-tuple-element.101), channel_id=1, source_target_pairs={{0,1},{1,2},{2,3},{3,0},{4,5},{5,6},{6,7},{7,4},{8,9},{9,10},{10,1... | collective-permute-start | bytes 1179656 | tf_op jit(solution)/shard_map/ppermute | solution.py:26
  63.5 14.3 %collective-permute-start.12 = (bf16[384,512]{1,0:T(8,128)(2,1)S(1)}, bf16[384,512]{1,0:T(8,128)(2,1)S(1)}, u32[]{:S(2)}, u32[]{:S(2)}) collective-permute-start(bf16[384,512]{1,0:T(8,128)(2,1)S(1)} %get-tuple-element.99), channel_id=1, source_target_pairs={{0,3},{1,0},{2,1},{3,2},{4,7},{5,4},{6,5},{7,6},{8,11},{9,8},{10,9... | collective-permute-start | bytes 1179656 | tf_op jit(solution)/shard_map/ppermute | solution.py:26
  65.0 14.2 %collective-permute-start.15 = (bf16[384,512]{1,0:T(8,128)(2,1)S(1)}, bf16[384,512]{1,0:T(8,128)(2,1)S(1)}, u32[]{:S(2)}, u32[]{:S(2)}) collective-permute-start(bf16[384,512]{1,0:T(8,128)(2,1)S(1)} %get-tuple-element.102), channel_id=1, source_target_pairs={{0,1},{1,2},{2,3},{3,0},{4,5},{5,6},{6,7},{7,4},{8,9},{9,10},{10,1... | collective-permute-start | bytes 1179656 | tf_op jit(solution)/shard_map/ppermute | solution.py:26
  69.5 16.7 %collective-permute-start.17 = (bf16[384,512]{1,0:T(8,128)(2,1)S(1)}, bf16[384,512]{1,0:T(8,128)(2,1)S(1)}, u32[]{:S(2)}, u32[]{:S(2)}) collective-permute-start(bf16[384,512]{1,0:T(8,128)(2,1)S(1)} %shard_map.183), channel_id=1, source_target_pairs={{0,3},{1,0},{2,1},{3,2},{4,7},{5,4},{6,5},{7,6},{8,11},{9,8},{10,9... | collective-permute-start | bytes 1179656 | tf_op jit(solution)/shard_map/ppermute | solution.py:26
  71.4 16.3 %collective-permute-start.14 = (bf16[384,512]{1,0:T(8,128)(2,1)S(1)}, bf16[384,512]{1,0:T(8,128)(2,1)S(1)}, u32[]{:S(2)}, u32[]{:S(2)}) collective-permute-start(bf16[384,512]{1,0:T(8,128)(2,1)S(1)} %shard_map.182), channel_id=1, source_target_pairs={{0,1},{1,2},{2,3},{3,0},{4,5},{5,6},{6,7},{7,4},{8,9},{9,10},{10,1... | collective-permute-start | bytes 1179656 | tf_op jit(solution)/shard_map/ppermute | solution.py:26
  89.0 30.8 %all-to-all-start.1 = ((bf16[64,48,128]{2,1,0:T(8,128)(2,1)}), bf16[64,48,128]{2,1,0:T(8,128)(2,1)S(1)}, u32[]{:S(2)}, u32[]{:S(2)}) async-start(bf16[64,48,128]{2,1,0:T(8,128)(2,1)} %bitcast.9), calls=%async_computation.1 | async-start | bytes 1572864 | tf_op jit(solution)/shard_map/all_to_all | solution.py:554
  120.3 7.2 %collective-permute-start.18 = (bf16[256,512]{1,0:T(8,128)(2,1)S(1)}, bf16[256,512]{1,0:T(8,128)(2,1)S(1)}, u32[]{:S(2)}, u32[]{:S(2)}) collective-permute-start(bf16[256,512]{1,0:T(8,128)(2,1)S(1)} %shard_map.186.own.refs_0_), channel_id=1, source_target_pairs={{0,3},{1,0},{2,1},{3,2},{4,7},{5,4},{6,5},{7,6},{8,11},{9,8},{10,9... | collective-permute-start | bytes 786440 | tf_op jit(solution)/shard_map/ppermute | solution.py:26
  120.3 8.3 %collective-permute-start.19 = (bf16[256,512]{1,0:T(8,128)(2,1)S(1)}, bf16[256,512]{1,0:T(8,128)(2,1)S(1)}, u32[]{:S(2)}, u32[]{:S(2)}) collective-permute-start(bf16[256,512]{1,0:T(8,128)(2,1)S(1)} %shard_map.186.own.refs_0_), channel_id=1, source_target_pairs={{0,1},{1,2},{2,3},{3,0},{4,5},{5,6},{6,7},{7,4},{8,9},{9,10},{10,1... | collective-permute-start | bytes 786440 | tf_op jit(solution)/shard_map/ppermute | solution.py:26
  130.4 14.1 %collective-permute-start.28 = (bf16[256,1536]{1,0:T(8,128)(2,1)}, bf16[256,1536]{1,0:T(8,128)(2,1)S(1)}, u32[]{:S(2)}, u32[]{:S(2)}) collective-permute-start(bf16[256,1536]{1,0:T(8,128)(2,1)} %get-tuple-element.128), channel_id=1, source_target_pairs={{0,4},{4,0},{1,5},{5,1},{2,6},{6,2},{3,7},{7,3},{8,12},{12,8},{9,1... | collective-permute-start | bytes 2359304 | tf_op jit(solution)/shard_map/ppermute | solution.py:26
  132.1 9.4 %collective-permute-start.20 = (bf16[256,512]{1,0:T(8,128)(2,1)S(1)}, bf16[256,512]{1,0:T(8,128)(2,1)S(1)}, u32[]{:S(2)}, u32[]{:S(2)}) collective-permute-start(bf16[256,512]{1,0:T(8,128)(2,1)S(1)} %shard_map.186.own.refs_0_), channel_id=1, source_target_pairs={{0,2},{1,3},{2,0},{3,1},{4,6},{5,7},{6,4},{7,5},{8,10},{9,11},{10,... | collective-permute-start | bytes 786440 | tf_op jit(solution)/shard_map/ppermute | solution.py:26
  145.9 9.1 %collective-permute-start.30 = (bf16[64,2048]{1,0:T(8,128)(2,1)S(1)}, bf16[64,2048]{1,0:T(8,128)(2,1)S(1)}, u32[]{:S(2)}, u32[]{:S(2)}) collective-permute-start(bf16[64,2048]{1,0:T(8,128)(2,1)S(1)} %get-tuple-element.132), channel_id=1, source_target_pairs={{0,16},{8,24},{16,0},{24,8},{1,17},{9,25},{17,1},{25,9},{2,18},{10... | collective-permute-start | bytes 786440 | tf_op jit(solution)/shard_map/ppermute | solution.py:26
  147.7 45.9 %collective-permute-start.26 = (bf16[768,512]{1,0:T(8,128)(2,1)}, bf16[768,512]{1,0:T(8,128)(2,1)}, u32[]{:S(2)}, u32[]{:S(2)}) collective-permute-start(bf16[768,512]{1,0:T(8,128)(2,1)} %get-tuple-element.123.refs_0_), channel_id=1, source_target_pairs={{0,3},{1,0},{2,1},{3,2},{4,7},{5,4},{6,5},{7,6},{8,11},{9,8},{10,9... | collective-permute-start | bytes 2359304 | tf_op jit(solution)/shard_map/ppermute | solution.py:26
  147.7 45.9 %collective-permute-start.27 = (bf16[768,512]{1,0:T(8,128)(2,1)}, bf16[768,512]{1,0:T(8,128)(2,1)}, u32[]{:S(2)}, u32[]{:S(2)}) collective-permute-start(bf16[768,512]{1,0:T(8,128)(2,1)} %get-tuple-element.123.refs_0_), channel_id=1, source_target_pairs={{0,1},{1,2},{2,3},{3,0},{4,5},{5,6},{6,7},{7,4},{8,9},{9,10},{10,1... | collective-permute-start | bytes 2359304 | tf_op jit(solution)/shard_map/ppermute | solution.py:26
  149.1 47.9 %collective-permute-start.25 = (bf16[768,512]{1,0:T(8,128)(2,1)}, bf16[768,512]{1,0:T(8,128)(2,1)S(1)}, u32[]{:S(2)}, u32[]{:S(2)}) collective-permute-start(bf16[768,512]{1,0:T(8,128)(2,1)} %get-tuple-element.123.refs_0_), channel_id=1, source_target_pairs={{0,2},{1,3},{2,0},{3,1},{4,6},{5,7},{6,4},{7,5},{8,10},{9,11},{10,... | collective-permute-start | bytes 2359304 | tf_op jit(solution)/shard_map/ppermute | solution.py:26
  149.8 11.5 %collective-permute-start.31 = (bf16[64,2048]{1,0:T(8,128)(2,1)S(1)}, bf16[64,2048]{1,0:T(8,128)(2,1)S(1)}, u32[]{:S(2)}, u32[]{:S(2)}) collective-permute-start(bf16[64,2048]{1,0:T(8,128)(2,1)S(1)} %get-tuple-element.133), channel_id=1, source_target_pairs={{0,8},{8,16},{16,24},{24,0},{1,9},{9,17},{17,25},{25,1},{2,10},{10... | collective-permute-start | bytes 786440 | tf_op jit(solution)/shard_map/ppermute | solution.py:26
  155.0 6.2 %collective-permute-start.32 = (bf16[64,2048]{1,0:T(8,128)(2,1)S(1)}, bf16[64,2048]{1,0:T(8,128)(2,1)S(1)}, u32[]{:S(2)}, u32[]{:S(2)}) collective-permute-start(bf16[64,2048]{1,0:T(8,128)(2,1)S(1)} %get-tuple-element.134), channel_id=1, source_target_pairs={{0,24},{8,0},{16,8},{24,16},{1,25},{9,1},{17,9},{25,17},{2,26},{10... | collective-permute-start | bytes 786440 | tf_op jit(solution)/shard_map/ppermute | solution.py:26
  162.1 40.9 %all-to-all-start.2 = ((bf16[8,8,2048]{2,1,0:T(8,128)(2,1)}), bf16[8,8,2048]{2,1,0:T(8,128)(2,1)S(1)}, u32[]{:S(2)}, u32[]{:S(2)}) async-start(bf16[8,8,2048]{2,1,0:T(8,128)(2,1)} %bitcast.17), calls=%async_computation.2 | async-start | bytes 524288 | tf_op jit(solution)/shard_map/all_to_all | solution.py:617
  168.8 16.5 %collective-permute-start.21 = (f32[8,256]{1,0:T(8,128)S(1)}, f32[8,256]{1,0:T(8,128)S(1)}, u32[]{:S(2)}, u32[]{:S(2)}) collective-permute-start(f32[8,256]{1,0:T(8,128)S(1)} %get-tuple-element.117.own), channel_id=1, source_target_pairs={{0,1},{1,2},{2,3},{3,0},{4,5},{5,6},{6,7},{7,4},{8,9},{9,10},{10,1... | collective-permute-start | bytes 24584 | tf_op jit(solution)/shard_map/ppermute | solution.py:26
  168.9 16.5 %collective-permute-start.22 = (f32[8,256]{1,0:T(8,128)S(1)}, f32[8,256]{1,0:T(8,128)S(1)}, u32[]{:S(2)}, u32[]{:S(2)}) collective-permute-start(f32[8,256]{1,0:T(8,128)S(1)} %get-tuple-element.117.own), channel_id=1, source_target_pairs={{0,3},{1,0},{2,1},{3,2},{4,7},{5,4},{6,5},{7,6},{8,11},{9,8},{10,9... | collective-permute-start | bytes 24584 | tf_op jit(solution)/shard_map/ppermute | solution.py:26
  189.7 10.9 %collective-permute-start.24 = (f32[32,512]{1,0:T(8,128)S(1)}, f32[32,512]{1,0:T(8,128)S(1)}, u32[]{:S(2)}, u32[]{:S(2)}) collective-permute-start(f32[32,512]{1,0:T(8,128)S(1)} %get-tuple-element.120), channel_id=1, source_target_pairs={{4,0},{8,4},{12,8},{16,12},{20,16},{24,20},{28,24},{32,28},{36,32}... | collective-permute-start | bytes 196616 | tf_op jit(solution)/shard_map/ppermute | solution.py:32
  (24 other events, 303.0 us)
where the time goes:
time: 204 us
  waiting for transfers between devices  93 us (46%)
  starting transfers between devices  63.7 us (31%)
  Pallas kernels  40.2 us (20%)
  local copies, waits for them, and re-layouts  5.77 us (3%)
    ppermute x32, waiting for transfers between devices, shifted(): lax.ppermute(value, axis, [(i, (i + steps) % count) for i in range(count)])  72.6 us
    pallas_call x25, Pallas kernels, kernel(): pl.pallas_call(body, out_shape=tuple(((pltpu.HBM if i in to_hbm else pltp...  37.7 us
    ppermute x32, starting transfers between devices, shifted(): lax.ppermute(value, axis, [(i, (i + steps) % count) for i in range(count)])  35.2 us
    all_to_all x1, waiting for transfers between devices, per_device(): lax.all_to_all(returning.reshape(experts, chunk_rows // experts, LANES),...  16.4 us
    all_to_all x1, starting transfers between devices, per_device(): lax.all_to_all(outgoing.reshape(experts, chunk_rows // experts, LANES), S...  13 us
    all_to_all x1, starting transfers between devices, per_device(): lax.all_to_all(returning.reshape(experts, chunk_rows // experts, LANES),...  7.77 us
    unnamed x40, local copies, waits for them, and re-layouts  4.86 us
  transfers between devices with their start and end apart: 36, of which 19 were waited for; matrix products, arithmetic and copies ran while one was open for 0% of the time, Pallas kernels for 15%

commit v1 on v0

--- a/solution.py
+++ b/solution.py
@@ -137,22 +137,17 @@
     lax.fori_loop(0, 3, step, 0)
 
 
-def partial_far_body(chunks_ref, far_ref, rows_ref, far_top, far_bot, scratch):
+def partial_act_body(chunks_ref, far_ref, next_ref, prev_ref, own_ref, *outs_scratch):
+    rows_ref, far_top, far_bot, next_top, next_bot, prev_top, prev_bot, own_out, scratch = outs_scratch
     n, width = rows_ref.shape
     half = n // 2
     rows = from_chunks(chunks_ref[...], scratch, n, width // LANES)
     rows_ref[...] = rows
-    value = dot(rows, far_ref[...], 1, 1).astype(bf16)
-    far_top[...] = value[:half]
-    far_bot[...] = value[half:]
-
-
-def partial_rest_body(rows_ref, next_ref, prev_ref, own_ref, *outs):
-    next_top, next_bot, prev_top, prev_bot, own_out, rows_out = outs
-    rows = rows_ref[...]
-    half = rows.shape[0] // 2
-    rows_out[...] = rows
-    for weight, top, bot in ((next_ref, next_top, next_bot), (prev_ref, prev_top, prev_bot)):
+    for weight, top, bot in (
+        (far_ref, far_top, far_bot),
+        (next_ref, next_top, next_bot),
+        (prev_ref, prev_top, prev_bot),
+    ):
         value = dot(rows, weight[...], 1, 1).astype(bf16)
         top[...] = value[:half]
         bot[...] = value[half:]
@@ -235,10 +230,7 @@
         out_ref[:, pl.ds(pl.multiple_of(at * size, size), size)] = value.astype(bf16)
 
 
-def down_far_body(at_ref, act_ref, rows_ref, near_ref, *refs):
-    *operands, out_ref, one, two, three, block, sem = refs
-    for operand, copy in zip(operands, (one, two, three)):
-        copy[...] = operand[...]
+def down_far_body(at_ref, act_ref, rows_ref, near_ref, out_ref, block, sem):
     size = rows_ref.shape[1]
     block[...] = dot(act_ref[...], rows_ref[...], 0, 0).astype(bf16)
     at = lax.rem(at_ref[0] + 2, out_ref.shape[1] // size)
@@ -259,11 +251,22 @@
         act = act_ref[...]
         for s, mix_ref in enumerate(mixes):
             value = dot(act, mix_ref[...], 0, 0).reshape(block // 8, columns, 2, 8, size)
-            for x in range(columns):
-                zero, one = (value[:, x, core].reshape(block, size) for core in range(2))
-                at = (slice(x * block, (x + 1) * block), slice(s * size, (s + 1) * size))
-                send_ref[at] = jnp.where(first, one, zero).astype(bf16)
-                keep_ref[at] = jnp.where(first, zero, one).astype(bf16)
+            at = slice(s * size, (s + 1) * size)
+
+            def store(core, out_ref, value=value, at=at):
+                for x in range(columns):
+                    half = value[:, x, core].reshape(block, size)
+                    out_ref[x * block : (x + 1) * block, at] = half.astype(bf16)
+
+            @pl.when(first)
+            def _():
+                store(1, send_ref)
+                store(0, keep_ref)
+
+            @pl.when(jnp.logical_not(first))
+            def _():
+                store(0, send_ref)
+                store(1, keep_ref)
 
     return body
 
@@ -482,13 +485,13 @@
         (struct((chunk_rows, LANES)), struct((2, tok_rows), jnp.int32)),
         route_ids.T, route_weight.T, cot_out,
         flops=4 * tok_rows * slot_rows * local_cols, scratch=(chunk_scratch,),
-        staged=(), to_hbm=(1,),
+        staged=(), to_hbm=(0, 1),
     )
     moved = lax.all_to_all(
         outgoing.reshape(experts, chunk_rows // experts, LANES), SP, 0, 0, tiled=True
     )
-    dest, conv_late, down_late, rows_late, gate_late, up_late, _ = lax.optimization_barrier(
-        (dest, conv_out, down_weight, rows_in, gate_weight, up_weight, outgoing)
+    dest, conv_late, down_late, rows_late, gate_late, up_late = lax.optimization_barrier(
+        (dest, conv_out, down_weight, rows_in, gate_weight, up_weight)
     )
 
     def down_block(shift):
@@ -503,7 +506,7 @@
         factors_body,
         (struct((slot_rows, hidden)),) * 3,
         rows_late, gate_late, up_late,
-        flops=4 * slot_rows * hidden * local_cols * ways, staged=(),
+        flops=4 * slot_rows * hidden * local_cols * ways,
     )
     (pick,) = kernel(
         pick_body, (struct((tok_rows, slot_rows)),), dest, flops=tok_rows * slot_rows * 8
@@ -518,18 +521,13 @@
         (moved, act, for_up, for_gate, pick, stats_in)
     )
 
-    rows_near, far_top, far_bot = kernel(
-        partial_far_body,
-        (struct((slot_rows, local_cols)),) + (struct((half, hidden)),) * 2,
-        moved.reshape(chunk_rows, LANES), down_far,
-        flops=2 * slot_rows * local_cols * hidden, scratch=(chunk_scratch,),
-    )
-    *rest, rows_cot = kernel(
-        partial_rest_body,
-        (struct((half, hidden)),) * 4
-        + (struct((slot_rows, hidden)), struct((slot_rows, local_cols))),
-        rows_near, down_next, down_prev, down_own,
-        flops=6 * slot_rows * local_cols * hidden, to_hbm=(5,),
+    rows_cot, far_top, far_bot, *rest = kernel(
+        partial_act_body,
+        (struct((slot_rows, local_cols)),) + (struct((half, hidden)),) * 6
+        + (struct((slot_rows, hidden)),),
+        moved.reshape(chunk_rows, LANES), down_far, down_next, down_prev, down_own,
+        flops=2 * slot_rows * local_cols * hidden * ways,
+        scratch=(chunk_scratch,), to_hbm=(0,),
     )
     act_terms = reduce_over_ring(far_top, far_bot, rest)
     d_gate, d_up, far_top, far_bot = kernel(
@@ -640,13 +638,11 @@
     )
     hbm = pl.BlockSpec(memory_space=pltpu.HBM)
     vmem = pl.BlockSpec(memory_space=pltpu.VMEM)
-    conv_operands = (taps, value_pre, gate_pre)
-    grad_down, *conv_operands = pl.pallas_call(
+    grad_down = pl.pallas_call(
         down_far_body,
-        out_shape=(struct((hidden, width)),)
-        + tuple(pltpu.VMEM(v.shape, v.dtype) for v in conv_operands),
-        in_specs=[pl.BlockSpec(memory_space=pltpu.SMEM), vmem, vmem, hbm, vmem, vmem, vmem],
-        out_specs=(hbm, vmem, vmem, vmem),
+        out_shape=struct((hidden, width)),
+        in_specs=[pl.BlockSpec(memory_space=pltpu.SMEM), vmem, vmem, hbm],
+        out_specs=hbm,
         scratch_shapes=[pltpu.VMEM((hidden, local_cols), bf16), pltpu.SemaphoreType.DMA],
         input_output_aliases={3: 0},
         cost_estimate=pl.CostEstimate(
@@ -656,7 +652,7 @@
         name="down_far",
     )(
         at_ref,
-        *(pltpu.with_memory_space_constraint(v, pltpu.HBM) for v in (act, rows_far, grad_down, *conv_operands)),
+        *(pltpu.with_memory_space_constraint(v, pltpu.HBM) for v in (act, rows_far, grad_down)),
     )
     reach = taps.shape[0]
     convolution_gradient, edge = kernel(
@@ -670,8 +666,9 @@
     grad_value, grad_gate = kernel(
         conv_body,
         (struct((tok_rows, local_cols)),) * 2,
-        convolution_gradient, following, *conv_operands,
+        convolution_gradient, following, taps, value_pre, gate_pre,
         flops=2 * reach * tok_rows * local_cols, limit=8, to_hbm=(0, 1),
+        staged=(0, 1),
         scratch=(
             pltpu.VMEM((tok_rows + edge.shape[0], local_cols), f32),
             pltpu.VMEM((8, tok_rows + 24, LANES), f32),

time: 204 us -> 213 us (1.044)
  waiting for transfers between devices: 93 us -> 96.8 us
  starting transfers between devices: 63.7 us -> 67.1 us
  local copies, waits for them, and re-layouts: 5.77 us -> 8.91 us
  Pallas kernels: 40.2 us -> 38 us
    ppermute x32, waiting for transfers between devices: 72.6 us -> 80.4 us  [shifted(): lax.ppermute(value, axis, [(i, (i + steps) % count) for i in range(count)])]
    all_to_all x1, starting transfers between devices: 7.77 us -> 14.1 us  [per_device(): lax.all_to_all(returning.reshape(experts, chunk_rows // experts, LANES),...]
    all_to_all x1, waiting for transfers between devices: 3.96 us -> 0.01 us  [per_device(): lax.all_to_all(outgoing.reshape(experts, chunk_rows // experts, LANES), S...]
    ppermute x32, starting transfers between devices: 35.2 us -> 32 us  [shifted(): lax.ppermute(value, axis, [(i, (i + steps) % count) for i in range(count)])]
    pallas_call x25 -> x24, Pallas kernels: 37.7 us -> 35.6 us  [kernel(): pl.pallas_call(body, out_shape=tuple(((pltpu.HBM if i in to_hbm else pltp...]
    unnamed x40 -> x42, local copies, waits for them, and re-layouts: 4.86 us -> 6.73 us
  transfers between devices with their start and end apart: 36 -> 36, of which waited for: 19 -> 20; matrix products, arithmetic and copies ran while one was open for 0% -> 1% of each run, Pallas kernels for 15% -> 12%
where the time goes in v1:
time: 213 us; the launch traced here: 212 us
  waiting for transfers between devices  96.8 us (45%)
  starting transfers between devices  67.1 us (32%)
  Pallas kernels  38 us (18%)
  local copies, waits for them, and re-layouts  8.91 us (4%)
    ppermute x32, waiting for transfers between devices, shifted(): lax.ppermute(value, axis, [(i, (i + steps) % count) for i in range(count)])  80.4 us
    pallas_call x24, Pallas kernels, kernel(): pl.pallas_call(body, out_shape=tuple(((pltpu.HBM if i in to_hbm else pltp...  35.6 us
    ppermute x32, starting transfers between devices, shifted(): lax.ppermute(value, axis, [(i, (i + steps) % count) for i in range(count)])  32 us
    all_to_all x1, waiting for transfers between devices, per_device(): lax.all_to_all(returning.reshape(experts, chunk_rows // experts, LANES),...  16.4 us
    all_to_all x1, starting transfers between devices, per_device(): lax.all_to_all(returning.reshape(experts, chunk_rows // experts, LANES),...  14.1 us
    all_to_all x1, starting transfers between devices, per_device(): lax.all_to_all(outgoing.reshape(experts, chunk_rows // experts, LANES), S...  13 us
    unnamed x42, local copies, waits for them, and re-layouts  6.73 us
    ppermute x1, starting transfers between devices, passed_along(): lax.ppermute(value, axis, [(source, source + steps) for source in range(l...  4.31 us
  transfers between devices with their start and end apart: 36, of which 20 were waited for; matrix products, arithmetic and copies ran while one was open for 1% of the time, Pallas kernels for 12%

profile of v1, /device:TPU:1, one launch (start us, length us, event | category | flops | bytes accessed | tf_op | source)
XLA Modules:
  0.0 211.8 jit_solution(18203204999793858738)
XLA Ops:
  0.7 2.9 %shard_map.172 = (bf16[3072,128]{1,0:T(8,128)(2,1)}, s32[2,256]{1,0:T(2,128)}) custom-call(s32[2,256]{1,0:T(2,128)} %bitcast.34, f32[2,256]{1,0:T(2,128)} %bitcast.35, bf16[256,512]{1,0:T(8,128)(2,1)} %cot_ref.3), custom_call_target="tpu_custom_call" | custom-call | flops 402653184 | bytes 1054720 | tf_op jit(solution)/shard_map/pallas_call | solution.py:46
  3.5 13.0 %all-to-all-start = ((bf16[64,48,128]{2,1,0:T(8,128)(2,1)}), bf16[64,48,128]{2,1,0:T(8,128)(2,1)S(1)}, u32[]{:S(2)}, u32[]{:S(2)}) async-start(bf16[64,48,128]{2,1,0:T(8,128)(2,1)} %bitcast.32), calls=%async_computation | async-start | bytes 1572864 | tf_op jit(solution)/shard_map/all_to_all | solution.py:490
  16.6 2.2 %constant_dynamic-slice_fusion = (bf16[256,512]{1,0:T(8,128)(2,1)}, bf16[256,512]{1,0:T(8,128)(2,1)}, bf16[256,512]{1,0:T(8,128)(2,1)}, bf16[256,512]{1,0:T(8,128)(2,1)}) fusion(bf16[256,2048]{1,0:T(8,128)(2,1)} %bitcast.31, s32[]{:T(128)S(6)} %select_n.38, s32[]{:T(128)S(6)} %select_n.36, s32[]{:T(128)S(6)} %select_n.34, s32[]{:T(128)S(6)} %select_n.32), kind=kLoop, calls=%fused_computation | loop fusion | bytes 2097168 | tf_op jit(solution)/shard_map/dynamic_slice | solution.py:499
  18.8 2.9 %collective-permute-start.3 = (bf16[256,512]{1,0:T(8,128)(2,1)}, bf16[256,512]{1,0:T(8,128)(2,1)}, u32[]{:S(2)}, u32[]{:S(2)}) collective-permute-start(bf16[256,512]{1,0:T(8,128)(2,1)} %get-tuple-element.135), channel_id=1, source_target_pairs={{0,2},{1,3},{2,0},{3,1},{4,6},{5,7},{6,4},{7,5},{8,10},{9,11},{10,... | collective-permute-start | bytes 786440 | tf_op jit(solution)/shard_map/ppermute | solution.py:26
  24.2 2.3 %collective-permute-start.1 = (f32[8,256]{1,0:T(8,128)S(1)}, f32[8,256]{1,0:T(8,128)S(1)}, u32[]{:S(2)}, u32[]{:S(2)}) collective-permute-start(f32[8,256]{1,0:T(8,128)S(1)} %shard_map.175.own), channel_id=1, source_target_pairs={{0,3},{1,0},{2,1},{3,2},{4,7},{5,4},{6,5},{7,6},{8,11},{9,8},{10,9... | collective-permute-start | bytes 24584 | tf_op jit(solution)/shard_map/ppermute | solution.py:26
  26.4 8.2 %collective-permute-done.one = f32[8,256]{1,0:T(8,128)S(1)} collective-permute-done((f32[8,256]{1,0:T(8,128)S(1)}, f32[8,256]{1,0:T(8,128)S(1)}, u32[]{:S(2)}, u32[]{:S(2)}) %collective-permute-start) | collective-permute-done | bytes 8224 | tf_op jit(solution)/shard_map/ppermute | solution.py:26
  34.6 2.9 %collective-permute-start.2 = (f32[8,256]{1,0:T(8,128)S(1)}, f32[8,256]{1,0:T(8,128)}, u32[]{:S(2)}, u32[]{:S(2)}) collective-permute-start(f32[8,256]{1,0:T(8,128)S(1)} %shard_map.175.own), channel_id=1, source_target_pairs={{0,2},{1,3},{2,0},{3,1},{4,6},{5,7},{6,4},{7,5},{8,10},{9,11},{10,... | collective-permute-start | bytes 24584 | tf_op jit(solution)/shard_map/ppermute | solution.py:26
  39.4 2.5 %shard_map.173 = (bf16[768,256]{1,0:T(8,128)(2,1)S(1)}, bf16[768,256]{1,0:T(8,128)(2,1)S(1)}, bf16[768,256]{1,0:T(8,128)(2,1)S(1)}) custom-call(bf16[768,2048]{1,0:T(8,128)(2,1)S(1)} %bitcast.28, bf16[2048,256]{1,0:T(8,128)(2,1)S(1)} %bitcast.21, bf16[2048,256]{1,0:T(8,128)(2,1)S(1)} %bitcast.24), custom_call_target="tpu_custom_call" | custom-call | flops 1610612736 | bytes 6422528 | tf_op jit(solution)/shard_map/pallas_call | solution.py:46
  44.3 2.8 %shard_map.176 = (bf16[768,512]{1,0:T(8,128)(2,1)}, bf16[384,256]{1,0:T(8,128)(2,1)S(1)}, bf16[384,256]{1,0:T(8,128)(2,1)S(1)}, bf16[384,256]{1,0:T(8,128)(2,1)S...) custom-call(bf16[3072,128]{1,0:T(8,128)(2,1)S(1)} %bitcast.27, ...), custom_call_target="tpu_custom_call" | custom-call | flops 805306368 | bytes 4194304 | tf_op jit(solution)/shard_map/pallas_call | solution.py:46
  50.0 2.8 %collective-permute-done.10.two_ref = bf16[384,256]{1,0:T(8,128)(2,1)S(1)} collective-permute-done((bf16[384,256]{1,0:T(8,128)(2,1)S(1)}, bf16[384,256]{1,0:T(8,128)(2,1)S(1)}, u32[]{:S(2)}, u32[]{:S(2)}) %collective-permute-start.10) | collective-permute-done | bytes 196640 | tf_op jit(solution)/shard_map/ppermute | solution.py:26
  54.7 2.3 %collective-permute-done.6.prev_top = bf16[384,256]{1,0:T(8,128)(2,1)S(1)} collective-permute-done((bf16[384,256]{1,0:T(8,128)(2,1)S(1)}, bf16[384,256]{1,0:T(8,128)(2,1)S(1)}, u32[]{:S(2)}, u32[]{:S(2)}) %collective-permute-start.6) | collective-permute-done | bytes 196640 | tf_op jit(solution)/shard_map/ppermute | solution.py:26
  57.9 3.3 %collective-permute-done.11.near_bot = bf16[384,256]{1,0:T(8,128)(2,1)S(1)} collective-permute-done((bf16[384,256]{1,0:T(8,128)(2,1)S(1)}, bf16[384,256]{1,0:T(8,128)(2,1)S(1)}, u32[]{:S(2)}, u32[]{:S(2)}) %collective-permute-start.11) | collective-permute-done | bytes 196640 | tf_op jit(solution)/shard_map/ppermute | solution.py:26
  66.6 2.9 %collective-permute-done.16.two_ref = bf16[384,512]{1,0:T(8,128)(2,1)S(1)} collective-permute-done((bf16[384,512]{1,0:T(8,128)(2,1)S(1)}, bf16[384,512]{1,0:T(8,128)(2,1)S(1)}, u32[]{:S(2)}, u32[]{:S(2)}) %collective-permute-start.16) | collective-permute-done | bytes 393248 | tf_op jit(solution)/shard_map/ppermute | solution.py:26
  72.4 5.5 %collective-permute-done.12.prev_top = bf16[384,512]{1,0:T(8,128)(2,1)S(1)} collective-permute-done((bf16[384,512]{1,0:T(8,128)(2,1)S(1)}, bf16[384,512]{1,0:T(8,128)(2,1)S(1)}, u32[]{:S(2)}, u32[]{:S(2)}) %collective-permute-start.12) | collective-permute-done | bytes 393248 | tf_op jit(solution)/shard_map/ppermute | solution.py:26
  79.2 7.1 %collective-permute-done.17.near_bot = bf16[384,512]{1,0:T(8,128)(2,1)S(1)} collective-permute-done((bf16[384,512]{1,0:T(8,128)(2,1)S(1)}, bf16[384,512]{1,0:T(8,128)(2,1)S(1)}, u32[]{:S(2)}, u32[]{:S(2)}) %collective-permute-start.17) | collective-permute-done | bytes 393248 | tf_op jit(solution)/shard_map/ppermute | solution.py:26
  89.0 14.1 %all-to-all-start.1 = ((bf16[64,48,128]{2,1,0:T(8,128)(2,1)}), bf16[64,48,128]{2,1,0:T(8,128)(2,1)S(1)}, u32[]{:S(2)}, u32[]{:S(2)}) async-start(bf16[64,48,128]{2,1,0:T(8,128)(2,1)} %bitcast.9), calls=%async_computation.1 | async-start | bytes 1572864 | tf_op jit(solution)/shard_map/all_to_all | solution.py:552
  105.1 4.7 %shard_map.184 = (bf16[2048,256]{1,0:T(8,128)(2,1)}, bf16[2048,256]{1,0:T(8,128)(2,1)}) custom-call(bf16[768,2048]{1,0:T(8,128)(2,1)S(1)} %bitcast.29, bf16[768,256]{1,0:T(8,128)(2,1)S(1)} %copy-done.15, bf16[768,256]{1,0:T(8,128)(2,1)S(1)} %copy-done.17), custom_call_target="tpu_custom_call" | custom-call | flops 1610612736 | bytes 6029312 | tf_op jit(solution)/shard_map/pallas_call | solution.py:46
  109.8 16.4 %all-to-all-done.1 = bf16[64,48,128]{2,1,0:T(8,128)(2,1)S(1)} async-done(((bf16[64,48,128]{2,1,0:T(8,128)(2,1)}), bf16[64,48,128]{2,1,0:T(8,128)(2,1)S(1)}, u32[]{:S(2)}, u32[]{:S(2)}) %all-to-all-start.1) | async-done | bytes 786464 | tf_op jit(solution)/shard_map/all_to_all | solution.py:552
  129.7 4.2 %collective-permute-done.18.following.refs_1_ = bf16[256,512]{1,0:T(8,128)(2,1)S(1)} collective-permute-done((bf16[256,512]{1,0:T(8,128)(2,1)S(1)}, bf16[256,512]{1,0:T(8,128)(2,1)S(1)}, u32[]{:S(2)}, u32[]{:S(2)}) %collective-permute-start.18) | collective-permute-done | bytes 262176 | tf_op jit(solution)/shard_map/ppermute | solution.py:26
  135.3 2.2 %shard_map.190 = (bf16[256,1536]{1,0:T(8,128)(2,1)}, bf16[256,1536]{1,0:T(8,128)(2,1)}) custom-call(s32[1]{0:T(128)} %bitcast.16.core_ref, bf16[256,512]{1,0:T(8,128)(2,1)S(1)} %get-tuple-element.119.act_ref, bf16[256,512]{1,0:T(8,128)(2,1)S(1)} %shard_map.185.own.refs_0_, bf16[256,512]{1,0:T(8,128)(2,1)S(1)} %collective-permute-done.18.following.refs_1_, ...), custom_call_target="tpu_custom_call" | custom-call | flops 402653184 | bytes 2621440 | tf_op jit(solution)/shard_map/pallas_call | solution.py:46
  139.5 9.2 %collective-permute-done.20.far.refs_0_ = bf16[256,512]{1,0:T(8,128)(2,1)S(1)} collective-permute-done((bf16[256,512]{1,0:T(8,128)(2,1)S(1)}, bf16[256,512]{1,0:T(8,128)(2,1)S(1)}, u32[]{:S(2)}, u32[]{:S(2)}) %collective-permute-start.20) | collective-permute-done | bytes 262176 | tf_op jit(solution)/shard_map/ppermute | solution.py:26
  156.6 5.8 %collective-permute-done.30.refs_1_ = bf16[64,2048]{1,0:T(8,128)(2,1)S(1)} collective-permute-done((bf16[64,2048]{1,0:T(8,128)(2,1)S(1)}, bf16[64,2048]{1,0:T(8,128)(2,1)S(1)}, u32[]{:S(2)}, u32[]{:S(2)}) %collective-permute-start.30) | collective-permute-done | bytes 262176 | tf_op jit(solution)/shard_map/ppermute | solution.py:26
  163.4 5.4 %collective-permute-done.31.refs_2_ = bf16[64,2048]{1,0:T(8,128)(2,1)S(1)} collective-permute-done((bf16[64,2048]{1,0:T(8,128)(2,1)S(1)}, bf16[64,2048]{1,0:T(8,128)(2,1)S(1)}, u32[]{:S(2)}, u32[]{:S(2)}) %collective-permute-start.31) | collective-permute-done | bytes 262176 | tf_op jit(solution)/shard_map/ppermute | solution.py:26
  169.7 3.7 %all-to-all-start.2 = ((bf16[8,8,2048]{2,1,0:T(8,128)(2,1)}), bf16[8,8,2048]{2,1,0:T(8,128)(2,1)S(1)}, u32[]{:S(2)}, u32[]{:S(2)}) async-start(bf16[8,8,2048]{2,1,0:T(8,128)(2,1)} %bitcast.17), calls=%async_computation.2 | async-start | bytes 524288 | tf_op jit(solution)/shard_map/all_to_all | solution.py:615
  173.4 2.8 %shard_map.187 = (f32[256,512]{1,0:T(8,128)S(1)}, f32[8,256]{1,0:T(8,128)S(1)}) custom-call(s32[1]{0:T(128)} %bitcast.at_ref, bf16[256,512]{1,0:T(8,128)(2,1)S(1)} %shard_map.185.own.refs_0_, bf16[256,512]{1,0:T(8,128)(2,1)S(1)} %collective-permute-done.18.following.refs_1_, bf16[256,512]{1,0:T(8,128)(2,1)S(1)} %collective-permute-done.19.previous.refs_2_, ...), custom_call_target="tpu_custom_call" | custom-call | flops 536870912 | bytes 4726784 | tf_op jit(solution)/shard_map/pallas_call | solution.py:46
  176.2 2.7 %collective-permute-start.22 = (f32[8,256]{1,0:T(8,128)S(1)}, f32[8,256]{1,0:T(8,128)S(1)}, u32[]{:S(2)}, u32[]{:S(2)}) collective-permute-start(f32[8,256]{1,0:T(8,128)S(1)} %get-tuple-element.111.own), channel_id=1, source_target_pairs={{0,3},{1,0},{2,1},{3,2},{4,7},{5,4},{6,5},{7,6},{8,11},{9,8},{10,9... | collective-permute-start | bytes 24584 | tf_op jit(solution)/shard_map/ppermute | solution.py:26
  178.9 13.3 %collective-permute-done.21.one = f32[8,256]{1,0:T(8,128)S(1)} collective-permute-done((f32[8,256]{1,0:T(8,128)S(1)}, f32[8,256]{1,0:T(8,128)S(1)}, u32[]{:S(2)}, u32[]{:S(2)}) %collective-permute-start.21) | collective-permute-done | bytes 8224 | tf_op jit(solution)/shard_map/ppermute | solution.py:26
  192.2 4.0 %collective-permute-done.23.three = f32[8,256]{1,0:T(8,128)S(1)} collective-permute-done((f32[8,256]{1,0:T(8,128)S(1)}, f32[8,256]{1,0:T(8,128)S(1)}, u32[]{:S(2)}, u32[]{:S(2)}) %collective-permute-start.23) | collective-permute-done | bytes 8224 | tf_op jit(solution)/shard_map/ppermute | solution.py:26
  196.5 4.3 %collective-permute-start.24 = (f32[32,512]{1,0:T(8,128)S(1)}, f32[32,512]{1,0:T(8,128)S(1)}, u32[]{:S(2)}, u32[]{:S(2)}) collective-permute-start(f32[32,512]{1,0:T(8,128)S(1)} %get-tuple-element.114), channel_id=1, source_target_pairs={{4,0},{8,4},{12,8},{16,12},{20,16},{24,20},{28,24},{32,28},{36,32}... | collective-permute-start | bytes 196616 | tf_op jit(solution)/shard_map/ppermute | solution.py:32
  200.9 3.5 %shard_map.189.near_ref = bf16[256,2048]{1,0:T(8,128)(2,1)} custom-call(s32[1]{0:T(128)} %bitcast.at_ref, bf16[768,256]{1,0:T(8,128)(2,1)} %copy-done, bf16[768,512]{1,0:T(8,128)(2,1)} %get-tuple-element.117.refs_0_, bf16[768,512]{1,0:T(8,128)(2,1)} %collective-permute-done.26.refs_1_, bf16[768,512]{1,0:T(8,128)(2,1)} %collective-permute-done.27.refs_2_), custom_call_target="tpu_custom_call" | custom-call | flops 603979776 | bytes 3801088 | tf_op jit(solution)/shard_map/pallas_call | solution.py:46
  205.3 2.4 %down_far.1 = bf16[256,2048]{1,0:T(8,128)(2,1)} custom-call(s32[1]{0:T(128)} %bitcast.at_ref, bf16[768,256]{1,0:T(8,128)(2,1)} %copy-done, bf16[768,512]{1,0:T(8,128)(2,1)} %copy-done.18, bf16[256,2048]{1,0:T(8,128)(2,1)} %shard_map.189.near_ref), custom_call_target="tpu_custom_call", output_to_operand_aliasing={{}: (3, {})} | custom-call | flops 201326592 | bytes 1048576 | tf_op jit(solution)/shard_map/down_far/pallas_call | solution.py:641
  207.7 3.5 %shard_map.195 = (bf16[256,512]{1,0:T(8,128)(2,1)}, bf16[256,512]{1,0:T(8,128)(2,1)}) custom-call(f32[256,512]{1,0:T(8,128)S(1)} %get-tuple-element.128.grad_ref, f32[32,512]{1,0:T(8,128)S(1)} %collective-permute-done.24.edge_ref, f32[31,512]{1,0:T(8,128)} %taps_ref.1, bf16[256,512]{1,0:T(8,128)(2,1)} %value_ref.1, bf16[256,512]{1,0:T(8,128)(2,1)} %gate_ref.1), custom_call_target="tpu_custom_call" | custom-call | flops 8126464 | bytes 1701888 | tf_op jit(solution)/shard_map/pallas_call | solution.py:46
  (108 shorter events, 45.2 us)
Async XLA Ops:
  3.5 40.6 %all-to-all-start = ((bf16[64,48,128]{2,1,0:T(8,128)(2,1)}), bf16[64,48,128]{2,1,0:T(8,128)(2,1)S(1)}, u32[]{:S(2)}, u32[]{:S(2)}) async-start(bf16[64,48,128]{2,1,0:T(8,128)(2,1)} %bitcast.32), calls=%async_computation | async-start | bytes 1572864 | tf_op jit(solution)/shard_map/all_to_all | solution.py:490
  18.8 25.4 %collective-permute-start.3 = (bf16[256,512]{1,0:T(8,128)(2,1)}, bf16[256,512]{1,0:T(8,128)(2,1)}, u32[]{:S(2)}, u32[]{:S(2)}) collective-permute-start(bf16[256,512]{1,0:T(8,128)(2,1)} %get-tuple-element.135), channel_id=1, source_target_pairs={{0,2},{1,3},{2,0},{3,1},{4,6},{5,7},{6,4},{7,5},{8,10},{9,11},{10,... | collective-permute-start | bytes 786440 | tf_op jit(solution)/shard_map/ppermute | solution.py:26
  21.7 22.6 %collective-permute-start.4 = (bf16[256,512]{1,0:T(8,128)(2,1)}, bf16[256,512]{1,0:T(8,128)(2,1)}, u32[]{:S(2)}, u32[]{:S(2)}) collective-permute-start(bf16[256,512]{1,0:T(8,128)(2,1)} %get-tuple-element.134), channel_id=1, source_target_pairs={{0,3},{1,0},{2,1},{3,2},{4,7},{5,4},{6,5},{7,6},{8,11},{9,8},{10,9... | collective-permute-start | bytes 786440 | tf_op jit(solution)/shard_map/ppermute | solution.py:26
  22.5 21.8 %collective-permute-start.5 = (bf16[256,512]{1,0:T(8,128)(2,1)}, bf16[256,512]{1,0:T(8,128)(2,1)}, u32[]{:S(2)}, u32[]{:S(2)}) collective-permute-start(bf16[256,512]{1,0:T(8,128)(2,1)} %get-tuple-element.133), channel_id=1, source_target_pairs={{0,1},{1,2},{2,3},{3,0},{4,5},{5,6},{6,7},{7,4},{8,9},{9,10},{10,1... | collective-permute-start | bytes 786440 | tf_op jit(solution)/shard_map/ppermute | solution.py:26
  23.7 10.9 %collective-permute-start = (f32[8,256]{1,0:T(8,128)S(1)}, f32[8,256]{1,0:T(8,128)S(1)}, u32[]{:S(2)}, u32[]{:S(2)}) collective-permute-start(f32[8,256]{1,0:T(8,128)S(1)} %shard_map.175.own), channel_id=1, source_target_pairs={{0,1},{1,2},{2,3},{3,0},{4,5},{5,6},{6,7},{7,4},{8,9},{9,10},{10,1... | collective-permute-start | bytes 24584 | tf_op jit(solution)/shard_map/ppermute | solution.py:26
  24.2 19.5 %collective-permute-start.1 = (f32[8,256]{1,0:T(8,128)S(1)}, f32[8,256]{1,0:T(8,128)S(1)}, u32[]{:S(2)}, u32[]{:S(2)}) collective-permute-start(f32[8,256]{1,0:T(8,128)S(1)} %shard_map.175.own), channel_id=1, source_target_pairs={{0,3},{1,0},{2,1},{3,2},{4,7},{5,4},{6,5},{7,6},{8,11},{9,8},{10,9... | collective-permute-start | bytes 24584 | tf_op jit(solution)/shard_map/ppermute | solution.py:26
  34.6 9.6 %collective-permute-start.2 = (f32[8,256]{1,0:T(8,128)S(1)}, f32[8,256]{1,0:T(8,128)}, u32[]{:S(2)}, u32[]{:S(2)}) collective-permute-start(f32[8,256]{1,0:T(8,128)S(1)} %shard_map.175.own), channel_id=1, source_target_pairs={{0,2},{1,3},{2,0},{3,1},{4,6},{5,7},{6,4},{7,5},{8,10},{9,11},{10,... | collective-permute-start | bytes 24584 | tf_op jit(solution)/shard_map/ppermute | solution.py:26
  48.5 8.5 %collective-permute-start.6 = (bf16[384,256]{1,0:T(8,128)(2,1)S(1)}, bf16[384,256]{1,0:T(8,128)(2,1)S(1)}, u32[]{:S(2)}, u32[]{:S(2)}) collective-permute-start(bf16[384,256]{1,0:T(8,128)(2,1)S(1)} %get-tuple-element.82), channel_id=1, source_target_pairs={{0,3},{1,0},{2,1},{3,2},{4,7},{5,4},{6,5},{7,6},{8,11},{9,8},{10,9... | collective-permute-start | bytes 589832 | tf_op jit(solution)/shard_map/ppermute | solution.py:26
  49.8 8.1 %collective-permute-start.9 = (bf16[384,256]{1,0:T(8,128)(2,1)S(1)}, bf16[384,256]{1,0:T(8,128)(2,1)S(1)}, u32[]{:S(2)}, u32[]{:S(2)}) collective-permute-start(bf16[384,256]{1,0:T(8,128)(2,1)S(1)} %get-tuple-element.85), channel_id=1, source_target_pairs={{0,1},{1,2},{2,3},{3,0},{4,5},{5,6},{6,7},{7,4},{8,9},{9,10},{10,1... | collective-permute-start | bytes 589832 | tf_op jit(solution)/shard_map/ppermute | solution.py:26
  52.9 8.4 %collective-permute-start.11 = (bf16[384,256]{1,0:T(8,128)(2,1)S(1)}, bf16[384,256]{1,0:T(8,128)(2,1)S(1)}, u32[]{:S(2)}, u32[]{:S(2)}) collective-permute-start(bf16[384,256]{1,0:T(8,128)(2,1)S(1)} %shard_map.178), channel_id=1, source_target_pairs={{0,3},{1,0},{2,1},{3,2},{4,7},{5,4},{6,5},{7,6},{8,11},{9,8},{10,9... | collective-permute-start | bytes 589832 | tf_op jit(solution)/shard_map/ppermute | solution.py:26
  53.5 7.9 %collective-permute-start.8 = (bf16[384,256]{1,0:T(8,128)(2,1)S(1)}, bf16[384,256]{1,0:T(8,128)(2,1)S(1)}, u32[]{:S(2)}, u32[]{:S(2)}) collective-permute-start(bf16[384,256]{1,0:T(8,128)(2,1)S(1)} %shard_map.177), channel_id=1, source_target_pairs={{0,1},{1,2},{2,3},{3,0},{4,5},{5,6},{6,7},{7,4},{8,9},{9,10},{10,1... | collective-permute-start | bytes 589832 | tf_op jit(solution)/shard_map/ppermute | solution.py:26
  62.1 7.4 %collective-permute-start.16 = (bf16[384,512]{1,0:T(8,128)(2,1)S(1)}, bf16[384,512]{1,0:T(8,128)(2,1)S(1)}, u32[]{:S(2)}, u32[]{:S(2)}) collective-permute-start(bf16[384,512]{1,0:T(8,128)(2,1)S(1)} %get-tuple-element.98), channel_id=1, source_target_pairs={{0,3},{1,0},{2,1},{3,2},{4,7},{5,4},{6,5},{7,6},{8,11},{9,8},{10,9... | collective-permute-start | bytes 1179656 | tf_op jit(solution)/shard_map/ppermute | solution.py:26
  62.2 9.0 %collective-permute-start.13 = (bf16[384,512]{1,0:T(8,128)(2,1)S(1)}, bf16[384,512]{1,0:T(8,128)(2,1)S(1)}, u32[]{:S(2)}, u32[]{:S(2)}) collective-permute-start(bf16[384,512]{1,0:T(8,128)(2,1)S(1)} %get-tuple-element.95), channel_id=1, source_target_pairs={{0,1},{1,2},{2,3},{3,0},{4,5},{5,6},{6,7},{7,4},{8,9},{9,10},{10,1... | collective-permute-start | bytes 1179656 | tf_op jit(solution)/shard_map/ppermute | solution.py:26
  65.1 12.8 %collective-permute-start.12 = (bf16[384,512]{1,0:T(8,128)(2,1)S(1)}, bf16[384,512]{1,0:T(8,128)(2,1)S(1)}, u32[]{:S(2)}, u32[]{:S(2)}) collective-permute-start(bf16[384,512]{1,0:T(8,128)(2,1)S(1)} %get-tuple-element.93), channel_id=1, source_target_pairs={{0,3},{1,0},{2,1},{3,2},{4,7},{5,4},{6,5},{7,6},{8,11},{9,8},{10,9... | collective-permute-start | bytes 1179656 | tf_op jit(solution)/shard_map/ppermute | solution.py:26
  66.5 12.8 %collective-permute-start.15 = (bf16[384,512]{1,0:T(8,128)(2,1)S(1)}, bf16[384,512]{1,0:T(8,128)(2,1)S(1)}, u32[]{:S(2)}, u32[]{:S(2)}) collective-permute-start(bf16[384,512]{1,0:T(8,128)(2,1)S(1)} %get-tuple-element.96), channel_id=1, source_target_pairs={{0,1},{1,2},{2,3},{3,0},{4,5},{5,6},{6,7},{7,4},{8,9},{9,10},{10,1... | collective-permute-start | bytes 1179656 | tf_op jit(solution)/shard_map/ppermute | solution.py:26
  69.6 16.7 %collective-permute-start.17 = (bf16[384,512]{1,0:T(8,128)(2,1)S(1)}, bf16[384,512]{1,0:T(8,128)(2,1)S(1)}, u32[]{:S(2)}, u32[]{:S(2)}) collective-permute-start(bf16[384,512]{1,0:T(8,128)(2,1)S(1)} %shard_map.182), channel_id=1, source_target_pairs={{0,3},{1,0},{2,1},{3,2},{4,7},{5,4},{6,5},{7,6},{8,11},{9,8},{10,9... | collective-permute-start | bytes 1179656 | tf_op jit(solution)/shard_map/ppermute | solution.py:26
  71.3 16.4 %collective-permute-start.14 = (bf16[384,512]{1,0:T(8,128)(2,1)S(1)}, bf16[384,512]{1,0:T(8,128)(2,1)S(1)}, u32[]{:S(2)}, u32[]{:S(2)}) collective-permute-start(bf16[384,512]{1,0:T(8,128)(2,1)S(1)} %shard_map.181), channel_id=1, source_target_pairs={{0,1},{1,2},{2,3},{3,0},{4,5},{5,6},{6,7},{7,4},{8,9},{9,10},{10,1... | collective-permute-start | bytes 1179656 | tf_op jit(solution)/shard_map/ppermute | solution.py:26
  89.0 37.1 %all-to-all-start.1 = ((bf16[64,48,128]{2,1,0:T(8,128)(2,1)}), bf16[64,48,128]{2,1,0:T(8,128)(2,1)S(1)}, u32[]{:S(2)}, u32[]{:S(2)}) async-start(bf16[64,48,128]{2,1,0:T(8,128)(2,1)} %bitcast.9), calls=%async_computation.1 | async-start | bytes 1572864 | tf_op jit(solution)/shard_map/all_to_all | solution.py:552
  126.6 7.2 %collective-permute-start.18 = (bf16[256,512]{1,0:T(8,128)(2,1)S(1)}, bf16[256,512]{1,0:T(8,128)(2,1)S(1)}, u32[]{:S(2)}, u32[]{:S(2)}) collective-permute-start(bf16[256,512]{1,0:T(8,128)(2,1)S(1)} %shard_map.185.own.refs_0_), channel_id=1, source_target_pairs={{0,3},{1,0},{2,1},{3,2},{4,7},{5,4},{6,5},{7,6},{8,11},{9,8},{10,9... | collective-permute-start | bytes 786440 | tf_op jit(solution)/shard_map/ppermute | solution.py:26
  127.2 8.1 %collective-permute-start.19 = (bf16[256,512]{1,0:T(8,128)(2,1)S(1)}, bf16[256,512]{1,0:T(8,128)(2,1)S(1)}, u32[]{:S(2)}, u32[]{:S(2)}) collective-permute-start(bf16[256,512]{1,0:T(8,128)(2,1)S(1)} %shard_map.185.own.refs_0_), channel_id=1, source_target_pairs={{0,1},{1,2},{2,3},{3,0},{4,5},{5,6},{6,7},{7,4},{8,9},{9,10},{10,1... | collective-permute-start | bytes 786440 | tf_op jit(solution)/shard_map/ppermute | solution.py:26
  137.5 14.3 %collective-permute-start.28 = (bf16[256,1536]{1,0:T(8,128)(2,1)}, bf16[256,1536]{1,0:T(8,128)(2,1)S(1)}, u32[]{:S(2)}, u32[]{:S(2)}) collective-permute-start(bf16[256,1536]{1,0:T(8,128)(2,1)} %get-tuple-element.121), channel_id=1, source_target_pairs={{0,4},{4,0},{1,5},{5,1},{2,6},{6,2},{3,7},{7,3},{8,12},{12,8},{9,1... | collective-permute-start | bytes 2359304 | tf_op jit(solution)/shard_map/ppermute | solution.py:26
  139.4 9.4 %collective-permute-start.20 = (bf16[256,512]{1,0:T(8,128)(2,1)S(1)}, bf16[256,512]{1,0:T(8,128)(2,1)S(1)}, u32[]{:S(2)}, u32[]{:S(2)}) collective-permute-start(bf16[256,512]{1,0:T(8,128)(2,1)S(1)} %shard_map.185.own.refs_0_), channel_id=1, source_target_pairs={{0,2},{1,3},{2,0},{3,1},{4,6},{5,7},{6,4},{7,5},{8,10},{9,11},{10,... | collective-permute-start | bytes 786440 | tf_op jit(solution)/shard_map/ppermute | solution.py:26
  153.3 9.1 %collective-permute-start.30 = (bf16[64,2048]{1,0:T(8,128)(2,1)S(1)}, bf16[64,2048]{1,0:T(8,128)(2,1)S(1)}, u32[]{:S(2)}, u32[]{:S(2)}) collective-permute-start(bf16[64,2048]{1,0:T(8,128)(2,1)S(1)} %get-tuple-element.125), channel_id=1, source_target_pairs={{0,16},{8,24},{16,0},{24,8},{1,17},{9,25},{17,1},{25,9},{2,18},{10... | collective-permute-start | bytes 786440 | tf_op jit(solution)/shard_map/ppermute | solution.py:26
  155.0 45.9 %collective-permute-start.26 = (bf16[768,512]{1,0:T(8,128)(2,1)}, bf16[768,512]{1,0:T(8,128)(2,1)}, u32[]{:S(2)}, u32[]{:S(2)}) collective-permute-start(bf16[768,512]{1,0:T(8,128)(2,1)} %get-tuple-element.117.refs_0_), channel_id=1, source_target_pairs={{0,3},{1,0},{2,1},{3,2},{4,7},{5,4},{6,5},{7,6},{8,11},{9,8},{10,9... | collective-permute-start | bytes 2359304 | tf_op jit(solution)/shard_map/ppermute | solution.py:26
  155.0 45.9 %collective-permute-start.27 = (bf16[768,512]{1,0:T(8,128)(2,1)}, bf16[768,512]{1,0:T(8,128)(2,1)}, u32[]{:S(2)}, u32[]{:S(2)}) collective-permute-start(bf16[768,512]{1,0:T(8,128)(2,1)} %get-tuple-element.117.refs_0_), channel_id=1, source_target_pairs={{0,1},{1,2},{2,3},{3,0},{4,5},{5,6},{6,7},{7,4},{8,9},{9,10},{10,1... | collective-permute-start | bytes 2359304 | tf_op jit(solution)/shard_map/ppermute | solution.py:26
  156.5 47.9 %collective-permute-start.25 = (bf16[768,512]{1,0:T(8,128)(2,1)}, bf16[768,512]{1,0:T(8,128)(2,1)S(1)}, u32[]{:S(2)}, u32[]{:S(2)}) collective-permute-start(bf16[768,512]{1,0:T(8,128)(2,1)} %get-tuple-element.117.refs_0_), channel_id=1, source_target_pairs={{0,2},{1,3},{2,0},{3,1},{4,6},{5,7},{6,4},{7,5},{8,10},{9,11},{10,... | collective-permute-start | bytes 2359304 | tf_op jit(solution)/shard_map/ppermute | solution.py:26
  156.6 12.2 %collective-permute-start.31 = (bf16[64,2048]{1,0:T(8,128)(2,1)S(1)}, bf16[64,2048]{1,0:T(8,128)(2,1)S(1)}, u32[]{:S(2)}, u32[]{:S(2)}) collective-permute-start(bf16[64,2048]{1,0:T(8,128)(2,1)S(1)} %get-tuple-element.126), channel_id=1, source_target_pairs={{0,8},{8,16},{16,24},{24,0},{1,9},{9,17},{17,25},{25,1},{2,10},{10... | collective-permute-start | bytes 786440 | tf_op jit(solution)/shard_map/ppermute | solution.py:26
  162.4 6.4 %collective-permute-start.32 = (bf16[64,2048]{1,0:T(8,128)(2,1)S(1)}, bf16[64,2048]{1,0:T(8,128)(2,1)S(1)}, u32[]{:S(2)}, u32[]{:S(2)}) collective-permute-start(bf16[64,2048]{1,0:T(8,128)(2,1)S(1)} %get-tuple-element.127), channel_id=1, source_target_pairs={{0,24},{8,0},{16,8},{24,16},{1,25},{9,1},{17,9},{25,17},{2,26},{10... | collective-permute-start | bytes 786440 | tf_op jit(solution)/shard_map/ppermute | solution.py:26
  169.7 41.5 %all-to-all-start.2 = ((bf16[8,8,2048]{2,1,0:T(8,128)(2,1)}), bf16[8,8,2048]{2,1,0:T(8,128)(2,1)S(1)}, u32[]{:S(2)}, u32[]{:S(2)}) async-start(bf16[8,8,2048]{2,1,0:T(8,128)(2,1)} %bitcast.17), calls=%async_computation.2 | async-start | bytes 524288 | tf_op jit(solution)/shard_map/all_to_all | solution.py:615
  176.2 16.0 %collective-permute-start.21 = (f32[8,256]{1,0:T(8,128)S(1)}, f32[8,256]{1,0:T(8,128)S(1)}, u32[]{:S(2)}, u32[]{:S(2)}) collective-permute-start(f32[8,256]{1,0:T(8,128)S(1)} %get-tuple-element.111.own), channel_id=1, source_target_pairs={{0,1},{1,2},{2,3},{3,0},{4,5},{5,6},{6,7},{7,4},{8,9},{9,10},{10,1... | collective-permute-start | bytes 24584 | tf_op jit(solution)/shard_map/ppermute | solution.py:26
  176.2 16.0 %collective-permute-start.22 = (f32[8,256]{1,0:T(8,128)S(1)}, f32[8,256]{1,0:T(8,128)S(1)}, u32[]{:S(2)}, u32[]{:S(2)}) collective-permute-start(f32[8,256]{1,0:T(8,128)S(1)} %get-tuple-element.111.own), channel_id=1, source_target_pairs={{0,3},{1,0},{2,1},{3,2},{4,7},{5,4},{6,5},{7,6},{8,11},{9,8},{10,9... | collective-permute-start | bytes 24584 | tf_op jit(solution)/shard_map/ppermute | solution.py:26
  196.5 11.1 %collective-permute-start.24 = (f32[32,512]{1,0:T(8,128)S(1)}, f32[32,512]{1,0:T(8,128)S(1)}, u32[]{:S(2)}, u32[]{:S(2)}) collective-permute-start(f32[32,512]{1,0:T(8,128)S(1)} %get-tuple-element.114), channel_id=1, source_target_pairs={{4,0},{8,4},{12,8},{16,12},{20,16},{24,20},{28,24},{32,28},{36,32}... | collective-permute-start | bytes 196616 | tf_op jit(solution)/shard_map/ppermute | solution.py:32
  (25 other events, 348.0 us)

commit v2 on v1

--- a/solution.py
+++ b/solution.py
@@ -251,22 +251,11 @@
         act = act_ref[...]
         for s, mix_ref in enumerate(mixes):
             value = dot(act, mix_ref[...], 0, 0).reshape(block // 8, columns, 2, 8, size)
-            at = slice(s * size, (s + 1) * size)
-
-            def store(core, out_ref, value=value, at=at):
-                for x in range(columns):
-                    half = value[:, x, core].reshape(block, size)
-                    out_ref[x * block : (x + 1) * block, at] = half.astype(bf16)
-
-            @pl.when(first)
-            def _():
-                store(1, send_ref)
-                store(0, keep_ref)
-
-            @pl.when(jnp.logical_not(first))
-            def _():
-                store(0, send_ref)
-                store(1, keep_ref)
+            for x in range(columns):
+                zero, one = (value[:, x, core].reshape(block, size) for core in range(2))
+                at = (slice(x * block, (x + 1) * block), slice(s * size, (s + 1) * size))
+                send_ref[at] = jnp.where(first, one, zero).astype(bf16)
+                keep_ref[at] = jnp.where(first, zero, one).astype(bf16)
 
     return body
 

time: 213 us -> 212 us (level)
  no operation moved by 1% of the time
where the time goes in v2:
time: 212 us; the launch traced here: 211 us
  waiting for transfers between devices  96.8 us (46%)
  starting transfers between devices  67.2 us (32%)
  Pallas kernels  37.5 us (18%)
  local copies, waits for them, and re-layouts  8.91 us (4%)
    ppermute x32, waiting for transfers between devices, shifted(): lax.ppermute(value, axis, [(i, (i + steps) % count) for i in range(count)])  80.4 us
    pallas_call x24, Pallas kernels, kernel(): pl.pallas_call(body, out_shape=tuple(((pltpu.HBM if i in to_hbm else pltp...  35.1 us
    ppermute x32, starting transfers between devices, shifted(): lax.ppermute(value, axis, [(i, (i + steps) % count) for i in range(count)])  32 us
    all_to_all x1, waiting for transfers between devices, per_device(): lax.all_to_all(returning.reshape(experts, chunk_rows // experts, LANES),...  16.4 us
    all_to_all x1, starting transfers between devices, per_device(): lax.all_to_all(returning.reshape(experts, chunk_rows // experts, LANES),...  14.1 us
    all_to_all x1, starting transfers between devices, per_device(): lax.all_to_all(outgoing.reshape(experts, chunk_rows // experts, LANES), S...  13 us
    unnamed x42, local copies, waits for them, and re-layouts  6.73 us
    ppermute x1, starting transfers between devices, passed_along(): lax.ppermute(value, axis, [(source, source + steps) for source in range(l...  4.31 us
  transfers between devices with their start and end apart: 36, of which 20 were waited for; matrix products, arithmetic and copies ran while one was open for 1% of the time, Pallas kernels for 12%

profile of v2, /device:TPU:1, one launch (start us, length us, event | category | flops | bytes accessed | tf_op | source)
XLA Modules:
  0.0 211.3 jit_solution(11067347228229197680)
XLA Ops:
  0.7 2.9 %shard_map.172 = (bf16[3072,128]{1,0:T(8,128)(2,1)}, s32[2,256]{1,0:T(2,128)}) custom-call(s32[2,256]{1,0:T(2,128)} %bitcast.34, f32[2,256]{1,0:T(2,128)} %bitcast.35, bf16[256,512]{1,0:T(8,128)(2,1)} %cot_ref.3), custom_call_target="tpu_custom_call" | custom-call | flops 402653184 | bytes 1054720 | tf_op jit(solution)/shard_map/pallas_call | solution.py:46
  3.5 13.0 %all-to-all-start = ((bf16[64,48,128]{2,1,0:T(8,128)(2,1)}), bf16[64,48,128]{2,1,0:T(8,128)(2,1)S(1)}, u32[]{:S(2)}, u32[]{:S(2)}) async-start(bf16[64,48,128]{2,1,0:T(8,128)(2,1)} %bitcast.32), calls=%async_computation | async-start | bytes 1572864 | tf_op jit(solution)/shard_map/all_to_all | solution.py:479
  16.6 2.2 %constant_dynamic-slice_fusion = (bf16[256,512]{1,0:T(8,128)(2,1)}, bf16[256,512]{1,0:T(8,128)(2,1)}, bf16[256,512]{1,0:T(8,128)(2,1)}, bf16[256,512]{1,0:T(8,128)(2,1)}) fusion(bf16[256,2048]{1,0:T(8,128)(2,1)} %bitcast.31, s32[]{:T(128)S(6)} %select_n.38, s32[]{:T(128)S(6)} %select_n.36, s32[]{:T(128)S(6)} %select_n.34, s32[]{:T(128)S(6)} %select_n.32), kind=kLoop, calls=%fused_computation | loop fusion | bytes 2097168 | tf_op jit(solution)/shard_map/dynamic_slice | solution.py:488
  18.8 2.9 %collective-permute-start.3 = (bf16[256,512]{1,0:T(8,128)(2,1)}, bf16[256,512]{1,0:T(8,128)(2,1)}, u32[]{:S(2)}, u32[]{:S(2)}) collective-permute-start(bf16[256,512]{1,0:T(8,128)(2,1)} %get-tuple-element.135), channel_id=1, source_target_pairs={{0,2},{1,3},{2,0},{3,1},{4,6},{5,7},{6,4},{7,5},{8,10},{9,11},{10,... | collective-permute-start | bytes 786440 | tf_op jit(solution)/shard_map/ppermute | solution.py:26
  24.2 2.3 %collective-permute-start.1 = (f32[8,256]{1,0:T(8,128)S(1)}, f32[8,256]{1,0:T(8,128)S(1)}, u32[]{:S(2)}, u32[]{:S(2)}) collective-permute-start(f32[8,256]{1,0:T(8,128)S(1)} %shard_map.175.own), channel_id=1, source_target_pairs={{0,3},{1,0},{2,1},{3,2},{4,7},{5,4},{6,5},{7,6},{8,11},{9,8},{10,9... | collective-permute-start | bytes 24584 | tf_op jit(solution)/shard_map/ppermute | solution.py:26
  26.4 8.2 %collective-permute-done.one = f32[8,256]{1,0:T(8,128)S(1)} collective-permute-done((f32[8,256]{1,0:T(8,128)S(1)}, f32[8,256]{1,0:T(8,128)S(1)}, u32[]{:S(2)}, u32[]{:S(2)}) %collective-permute-start) | collective-permute-done | bytes 8224 | tf_op jit(solution)/shard_map/ppermute | solution.py:26
  34.6 2.9 %collective-permute-start.2 = (f32[8,256]{1,0:T(8,128)S(1)}, f32[8,256]{1,0:T(8,128)}, u32[]{:S(2)}, u32[]{:S(2)}) collective-permute-start(f32[8,256]{1,0:T(8,128)S(1)} %shard_map.175.own), channel_id=1, source_target_pairs={{0,2},{1,3},{2,0},{3,1},{4,6},{5,7},{6,4},{7,5},{8,10},{9,11},{10,... | collective-permute-start | bytes 24584 | tf_op jit(solution)/shard_map/ppermute | solution.py:26
  37.5 1.9 copy-done.12
  39.4 2.5 %shard_map.173 = (bf16[768,256]{1,0:T(8,128)(2,1)S(1)}, bf16[768,256]{1,0:T(8,128)(2,1)S(1)}, bf16[768,256]{1,0:T(8,128)(2,1)S(1)}) custom-call(bf16[768,2048]{1,0:T(8,128)(2,1)S(1)} %bitcast.28, bf16[2048,256]{1,0:T(8,128)(2,1)S(1)} %bitcast.21, bf16[2048,256]{1,0:T(8,128)(2,1)S(1)} %bitcast.24), custom_call_target="tpu_custom_call" | custom-call | flops 1610612736 | bytes 6422528 | tf_op jit(solution)/shard_map/pallas_call | solution.py:46
  44.3 2.8 %shard_map.176 = (bf16[768,512]{1,0:T(8,128)(2,1)}, bf16[384,256]{1,0:T(8,128)(2,1)S(1)}, bf16[384,256]{1,0:T(8,128)(2,1)S(1)}, bf16[384,256]{1,0:T(8,128)(2,1)S...) custom-call(bf16[3072,128]{1,0:T(8,128)(2,1)S(1)} %bitcast.27, ...), custom_call_target="tpu_custom_call" | custom-call | flops 805306368 | bytes 4194304 | tf_op jit(solution)/shard_map/pallas_call | solution.py:46
  50.0 2.8 %collective-permute-done.10.two_ref = bf16[384,256]{1,0:T(8,128)(2,1)S(1)} collective-permute-done((bf16[384,256]{1,0:T(8,128)(2,1)S(1)}, bf16[384,256]{1,0:T(8,128)(2,1)S(1)}, u32[]{:S(2)}, u32[]{:S(2)}) %collective-permute-start.10) | collective-permute-done | bytes 196640 | tf_op jit(solution)/shard_map/ppermute | solution.py:26
  54.7 2.3 %collective-permute-done.6.prev_top = bf16[384,256]{1,0:T(8,128)(2,1)S(1)} collective-permute-done((bf16[384,256]{1,0:T(8,128)(2,1)S(1)}, bf16[384,256]{1,0:T(8,128)(2,1)S(1)}, u32[]{:S(2)}, u32[]{:S(2)}) %collective-permute-start.6) | collective-permute-done | bytes 196640 | tf_op jit(solution)/shard_map/ppermute | solution.py:26
  57.9 3.3 %collective-permute-done.11.near_bot = bf16[384,256]{1,0:T(8,128)(2,1)S(1)} collective-permute-done((bf16[384,256]{1,0:T(8,128)(2,1)S(1)}, bf16[384,256]{1,0:T(8,128)(2,1)S(1)}, u32[]{:S(2)}, u32[]{:S(2)}) %collective-permute-start.11) | collective-permute-done | bytes 196640 | tf_op jit(solution)/shard_map/ppermute | solution.py:26
  66.6 2.9 %collective-permute-done.16.two_ref = bf16[384,512]{1,0:T(8,128)(2,1)S(1)} collective-permute-done((bf16[384,512]{1,0:T(8,128)(2,1)S(1)}, bf16[384,512]{1,0:T(8,128)(2,1)S(1)}, u32[]{:S(2)}, u32[]{:S(2)}) %collective-permute-start.16) | collective-permute-done | bytes 393248 | tf_op jit(solution)/shard_map/ppermute | solution.py:26
  72.4 5.5 %collective-permute-done.12.prev_top = bf16[384,512]{1,0:T(8,128)(2,1)S(1)} collective-permute-done((bf16[384,512]{1,0:T(8,128)(2,1)S(1)}, bf16[384,512]{1,0:T(8,128)(2,1)S(1)}, u32[]{:S(2)}, u32[]{:S(2)}) %collective-permute-start.12) | collective-permute-done | bytes 393248 | tf_op jit(solution)/shard_map/ppermute | solution.py:26
  79.2 7.1 %collective-permute-done.17.near_bot = bf16[384,512]{1,0:T(8,128)(2,1)S(1)} collective-permute-done((bf16[384,512]{1,0:T(8,128)(2,1)S(1)}, bf16[384,512]{1,0:T(8,128)(2,1)S(1)}, u32[]{:S(2)}, u32[]{:S(2)}) %collective-permute-start.17) | collective-permute-done | bytes 393248 | tf_op jit(solution)/shard_map/ppermute | solution.py:26
  89.0 14.1 %all-to-all-start.1 = ((bf16[64,48,128]{2,1,0:T(8,128)(2,1)}), bf16[64,48,128]{2,1,0:T(8,128)(2,1)S(1)}, u32[]{:S(2)}, u32[]{:S(2)}) async-start(bf16[64,48,128]{2,1,0:T(8,128)(2,1)} %bitcast.9), calls=%async_computation.1 | async-start | bytes 1572864 | tf_op jit(solution)/shard_map/all_to_all | solution.py:541
  105.1 4.7 %shard_map.184 = (bf16[2048,256]{1,0:T(8,128)(2,1)}, bf16[2048,256]{1,0:T(8,128)(2,1)}) custom-call(bf16[768,2048]{1,0:T(8,128)(2,1)S(1)} %bitcast.29, bf16[768,256]{1,0:T(8,128)(2,1)S(1)} %copy-done.15, bf16[768,256]{1,0:T(8,128)(2,1)S(1)} %copy-done.17), custom_call_target="tpu_custom_call" | custom-call | flops 1610612736 | bytes 6029312 | tf_op jit(solution)/shard_map/pallas_call | solution.py:46
  109.8 16.4 %all-to-all-done.1 = bf16[64,48,128]{2,1,0:T(8,128)(2,1)S(1)} async-done(((bf16[64,48,128]{2,1,0:T(8,128)(2,1)}), bf16[64,48,128]{2,1,0:T(8,128)(2,1)S(1)}, u32[]{:S(2)}, u32[]{:S(2)}) %all-to-all-start.1) | async-done | bytes 786464 | tf_op jit(solution)/shard_map/all_to_all | solution.py:541
  129.7 4.2 %collective-permute-done.18.following.refs_1_ = bf16[256,512]{1,0:T(8,128)(2,1)S(1)} collective-permute-done((bf16[256,512]{1,0:T(8,128)(2,1)S(1)}, bf16[256,512]{1,0:T(8,128)(2,1)S(1)}, u32[]{:S(2)}, u32[]{:S(2)}) %collective-permute-start.18) | collective-permute-done | bytes 262176 | tf_op jit(solution)/shard_map/ppermute | solution.py:26
  139.1 9.2 %collective-permute-done.20.far.refs_0_ = bf16[256,512]{1,0:T(8,128)(2,1)S(1)} collective-permute-done((bf16[256,512]{1,0:T(8,128)(2,1)S(1)}, bf16[256,512]{1,0:T(8,128)(2,1)S(1)}, u32[]{:S(2)}, u32[]{:S(2)}) %collective-permute-start.20) | collective-permute-done | bytes 262176 | tf_op jit(solution)/shard_map/ppermute | solution.py:26
  156.1 5.8 %collective-permute-done.30.refs_1_ = bf16[64,2048]{1,0:T(8,128)(2,1)S(1)} collective-permute-done((bf16[64,2048]{1,0:T(8,128)(2,1)S(1)}, bf16[64,2048]{1,0:T(8,128)(2,1)S(1)}, u32[]{:S(2)}, u32[]{:S(2)}) %collective-permute-start.30) | collective-permute-done | bytes 262176 | tf_op jit(solution)/shard_map/ppermute | solution.py:26
  162.9 5.4 %collective-permute-done.31.refs_2_ = bf16[64,2048]{1,0:T(8,128)(2,1)S(1)} collective-permute-done((bf16[64,2048]{1,0:T(8,128)(2,1)S(1)}, bf16[64,2048]{1,0:T(8,128)(2,1)S(1)}, u32[]{:S(2)}, u32[]{:S(2)}) %collective-permute-start.31) | collective-permute-done | bytes 262176 | tf_op jit(solution)/shard_map/ppermute | solution.py:26
  169.1 3.7 %all-to-all-start.2 = ((bf16[8,8,2048]{2,1,0:T(8,128)(2,1)}), bf16[8,8,2048]{2,1,0:T(8,128)(2,1)S(1)}, u32[]{:S(2)}, u32[]{:S(2)}) async-start(bf16[8,8,2048]{2,1,0:T(8,128)(2,1)} %bitcast.17), calls=%async_computation.2 | async-start | bytes 524288 | tf_op jit(solution)/shard_map/all_to_all | solution.py:604
  172.9 2.8 %shard_map.187 = (f32[256,512]{1,0:T(8,128)S(1)}, f32[8,256]{1,0:T(8,128)S(1)}) custom-call(s32[1]{0:T(128)} %bitcast.at_ref, bf16[256,512]{1,0:T(8,128)(2,1)S(1)} %shard_map.185.own.refs_0_, bf16[256,512]{1,0:T(8,128)(2,1)S(1)} %collective-permute-done.18.following.refs_1_, bf16[256,512]{1,0:T(8,128)(2,1)S(1)} %collective-permute-done.19.previous.refs_2_, ...), custom_call_target="tpu_custom_call" | custom-call | flops 536870912 | bytes 4726784 | tf_op jit(solution)/shard_map/pallas_call | solution.py:46
  175.7 2.7 %collective-permute-start.22 = (f32[8,256]{1,0:T(8,128)S(1)}, f32[8,256]{1,0:T(8,128)S(1)}, u32[]{:S(2)}, u32[]{:S(2)}) collective-permute-start(f32[8,256]{1,0:T(8,128)S(1)} %get-tuple-element.111.own), channel_id=1, source_target_pairs={{0,3},{1,0},{2,1},{3,2},{4,7},{5,4},{6,5},{7,6},{8,11},{9,8},{10,9... | collective-permute-start | bytes 24584 | tf_op jit(solution)/shard_map/ppermute | solution.py:26
  178.4 13.3 %collective-permute-done.21.one = f32[8,256]{1,0:T(8,128)S(1)} collective-permute-done((f32[8,256]{1,0:T(8,128)S(1)}, f32[8,256]{1,0:T(8,128)S(1)}, u32[]{:S(2)}, u32[]{:S(2)}) %collective-permute-start.21) | collective-permute-done | bytes 8224 | tf_op jit(solution)/shard_map/ppermute | solution.py:26
  191.7 4.0 %collective-permute-done.23.three = f32[8,256]{1,0:T(8,128)S(1)} collective-permute-done((f32[8,256]{1,0:T(8,128)S(1)}, f32[8,256]{1,0:T(8,128)S(1)}, u32[]{:S(2)}, u32[]{:S(2)}) %collective-permute-start.23) | collective-permute-done | bytes 8224 | tf_op jit(solution)/shard_map/ppermute | solution.py:26
  196.0 4.3 %collective-permute-start.24 = (f32[32,512]{1,0:T(8,128)S(1)}, f32[32,512]{1,0:T(8,128)S(1)}, u32[]{:S(2)}, u32[]{:S(2)}) collective-permute-start(f32[32,512]{1,0:T(8,128)S(1)} %get-tuple-element.114), channel_id=1, source_target_pairs={{4,0},{8,4},{12,8},{16,12},{20,16},{24,20},{28,24},{32,28},{36,32}... | collective-permute-start | bytes 196616 | tf_op jit(solution)/shard_map/ppermute | solution.py:32
  200.4 3.5 %shard_map.189.near_ref = bf16[256,2048]{1,0:T(8,128)(2,1)} custom-call(s32[1]{0:T(128)} %bitcast.at_ref, bf16[768,256]{1,0:T(8,128)(2,1)} %copy-done, bf16[768,512]{1,0:T(8,128)(2,1)} %get-tuple-element.117.refs_0_, bf16[768,512]{1,0:T(8,128)(2,1)} %collective-permute-done.26.refs_1_, bf16[768,512]{1,0:T(8,128)(2,1)} %collective-permute-done.27.refs_2_), custom_call_target="tpu_custom_call" | custom-call | flops 603979776 | bytes 3801088 | tf_op jit(solution)/shard_map/pallas_call | solution.py:46
  204.8 2.4 %down_far.1 = bf16[256,2048]{1,0:T(8,128)(2,1)} custom-call(s32[1]{0:T(128)} %bitcast.at_ref, bf16[768,256]{1,0:T(8,128)(2,1)} %copy-done, bf16[768,512]{1,0:T(8,128)(2,1)} %copy-done.18, bf16[256,2048]{1,0:T(8,128)(2,1)} %shard_map.189.near_ref), custom_call_target="tpu_custom_call", output_to_operand_aliasing={{}: (3, {})} | custom-call | flops 201326592 | bytes 1048576 | tf_op jit(solution)/shard_map/down_far/pallas_call | solution.py:630
  207.2 3.5 %shard_map.195 = (bf16[256,512]{1,0:T(8,128)(2,1)}, bf16[256,512]{1,0:T(8,128)(2,1)}) custom-call(f32[256,512]{1,0:T(8,128)S(1)} %get-tuple-element.128.grad_ref, f32[32,512]{1,0:T(8,128)S(1)} %collective-permute-done.24.edge_ref, f32[31,512]{1,0:T(8,128)} %taps_ref.1, bf16[256,512]{1,0:T(8,128)(2,1)} %value_ref.1, bf16[256,512]{1,0:T(8,128)(2,1)} %gate_ref.1), custom_call_target="tpu_custom_call" | custom-call | flops 8126464 | bytes 1701888 | tf_op jit(solution)/shard_map/pallas_call | solution.py:46
  (108 shorter events, 45.0 us)
Async XLA Ops:
  3.5 40.6 %all-to-all-start = ((bf16[64,48,128]{2,1,0:T(8,128)(2,1)}), bf16[64,48,128]{2,1,0:T(8,128)(2,1)S(1)}, u32[]{:S(2)}, u32[]{:S(2)}) async-start(bf16[64,48,128]{2,1,0:T(8,128)(2,1)} %bitcast.32), calls=%async_computation | async-start | bytes 1572864 | tf_op jit(solution)/shard_map/all_to_all | solution.py:479
  18.8 25.4 %collective-permute-start.3 = (bf16[256,512]{1,0:T(8,128)(2,1)}, bf16[256,512]{1,0:T(8,128)(2,1)}, u32[]{:S(2)}, u32[]{:S(2)}) collective-permute-start(bf16[256,512]{1,0:T(8,128)(2,1)} %get-tuple-element.135), channel_id=1, source_target_pairs={{0,2},{1,3},{2,0},{3,1},{4,6},{5,7},{6,4},{7,5},{8,10},{9,11},{10,... | collective-permute-start | bytes 786440 | tf_op jit(solution)/shard_map/ppermute | solution.py:26
  21.7 22.6 %collective-permute-start.4 = (bf16[256,512]{1,0:T(8,128)(2,1)}, bf16[256,512]{1,0:T(8,128)(2,1)}, u32[]{:S(2)}, u32[]{:S(2)}) collective-permute-start(bf16[256,512]{1,0:T(8,128)(2,1)} %get-tuple-element.134), channel_id=1, source_target_pairs={{0,3},{1,0},{2,1},{3,2},{4,7},{5,4},{6,5},{7,6},{8,11},{9,8},{10,9... | collective-permute-start | bytes 786440 | tf_op jit(solution)/shard_map/ppermute | solution.py:26
  22.5 21.8 %collective-permute-start.5 = (bf16[256,512]{1,0:T(8,128)(2,1)}, bf16[256,512]{1,0:T(8,128)(2,1)}, u32[]{:S(2)}, u32[]{:S(2)}) collective-permute-start(bf16[256,512]{1,0:T(8,128)(2,1)} %get-tuple-element.133), channel_id=1, source_target_pairs={{0,1},{1,2},{2,3},{3,0},{4,5},{5,6},{6,7},{7,4},{8,9},{9,10},{10,1... | collective-permute-start | bytes 786440 | tf_op jit(solution)/shard_map/ppermute | solution.py:26
  23.7 10.9 %collective-permute-start = (f32[8,256]{1,0:T(8,128)S(1)}, f32[8,256]{1,0:T(8,128)S(1)}, u32[]{:S(2)}, u32[]{:S(2)}) collective-permute-start(f32[8,256]{1,0:T(8,128)S(1)} %shard_map.175.own), channel_id=1, source_target_pairs={{0,1},{1,2},{2,3},{3,0},{4,5},{5,6},{6,7},{7,4},{8,9},{9,10},{10,1... | collective-permute-start | bytes 24584 | tf_op jit(solution)/shard_map/ppermute | solution.py:26
  24.2 19.5 %collective-permute-start.1 = (f32[8,256]{1,0:T(8,128)S(1)}, f32[8,256]{1,0:T(8,128)S(1)}, u32[]{:S(2)}, u32[]{:S(2)}) collective-permute-start(f32[8,256]{1,0:T(8,128)S(1)} %shard_map.175.own), channel_id=1, source_target_pairs={{0,3},{1,0},{2,1},{3,2},{4,7},{5,4},{6,5},{7,6},{8,11},{9,8},{10,9... | collective-permute-start | bytes 24584 | tf_op jit(solution)/shard_map/ppermute | solution.py:26
  34.6 9.6 %collective-permute-start.2 = (f32[8,256]{1,0:T(8,128)S(1)}, f32[8,256]{1,0:T(8,128)}, u32[]{:S(2)}, u32[]{:S(2)}) collective-permute-start(f32[8,256]{1,0:T(8,128)S(1)} %shard_map.175.own), channel_id=1, source_target_pairs={{0,2},{1,3},{2,0},{3,1},{4,6},{5,7},{6,4},{7,5},{8,10},{9,11},{10,... | collective-permute-start | bytes 24584 | tf_op jit(solution)/shard_map/ppermute | solution.py:26
  48.5 8.5 %collective-permute-start.6 = (bf16[384,256]{1,0:T(8,128)(2,1)S(1)}, bf16[384,256]{1,0:T(8,128)(2,1)S(1)}, u32[]{:S(2)}, u32[]{:S(2)}) collective-permute-start(bf16[384,256]{1,0:T(8,128)(2,1)S(1)} %get-tuple-element.82), channel_id=1, source_target_pairs={{0,3},{1,0},{2,1},{3,2},{4,7},{5,4},{6,5},{7,6},{8,11},{9,8},{10,9... | collective-permute-start | bytes 589832 | tf_op jit(solution)/shard_map/ppermute | solution.py:26
  49.8 8.1 %collective-permute-start.9 = (bf16[384,256]{1,0:T(8,128)(2,1)S(1)}, bf16[384,256]{1,0:T(8,128)(2,1)S(1)}, u32[]{:S(2)}, u32[]{:S(2)}) collective-permute-start(bf16[384,256]{1,0:T(8,128)(2,1)S(1)} %get-tuple-element.85), channel_id=1, source_target_pairs={{0,1},{1,2},{2,3},{3,0},{4,5},{5,6},{6,7},{7,4},{8,9},{9,10},{10,1... | collective-permute-start | bytes 589832 | tf_op jit(solution)/shard_map/ppermute | solution.py:26
  52.9 8.4 %collective-permute-start.11 = (bf16[384,256]{1,0:T(8,128)(2,1)S(1)}, bf16[384,256]{1,0:T(8,128)(2,1)S(1)}, u32[]{:S(2)}, u32[]{:S(2)}) collective-permute-start(bf16[384,256]{1,0:T(8,128)(2,1)S(1)} %shard_map.178), channel_id=1, source_target_pairs={{0,3},{1,0},{2,1},{3,2},{4,7},{5,4},{6,5},{7,6},{8,11},{9,8},{10,9... | collective-permute-start | bytes 589832 | tf_op jit(solution)/shard_map/ppermute | solution.py:26
  53.5 7.9 %collective-permute-start.8 = (bf16[384,256]{1,0:T(8,128)(2,1)S(1)}, bf16[384,256]{1,0:T(8,128)(2,1)S(1)}, u32[]{:S(2)}, u32[]{:S(2)}) collective-permute-start(bf16[384,256]{1,0:T(8,128)(2,1)S(1)} %shard_map.177), channel_id=1, source_target_pairs={{0,1},{1,2},{2,3},{3,0},{4,5},{5,6},{6,7},{7,4},{8,9},{9,10},{10,1... | collective-permute-start | bytes 589832 | tf_op jit(solution)/shard_map/ppermute | solution.py:26
  62.1 7.4 %collective-permute-start.16 = (bf16[384,512]{1,0:T(8,128)(2,1)S(1)}, bf16[384,512]{1,0:T(8,128)(2,1)S(1)}, u32[]{:S(2)}, u32[]{:S(2)}) collective-permute-start(bf16[384,512]{1,0:T(8,128)(2,1)S(1)} %get-tuple-element.98), channel_id=1, source_target_pairs={{0,3},{1,0},{2,1},{3,2},{4,7},{5,4},{6,5},{7,6},{8,11},{9,8},{10,9... | collective-permute-start | bytes 1179656 | tf_op jit(solution)/shard_map/ppermute | solution.py:26
  62.2 9.0 %collective-permute-start.13 = (bf16[384,512]{1,0:T(8,128)(2,1)S(1)}, bf16[384,512]{1,0:T(8,128)(2,1)S(1)}, u32[]{:S(2)}, u32[]{:S(2)}) collective-permute-start(bf16[384,512]{1,0:T(8,128)(2,1)S(1)} %get-tuple-element.95), channel_id=1, source_target_pairs={{0,1},{1,2},{2,3},{3,0},{4,5},{5,6},{6,7},{7,4},{8,9},{9,10},{10,1... | collective-permute-start | bytes 1179656 | tf_op jit(solution)/shard_map/ppermute | solution.py:26
  65.1 12.8 %collective-permute-start.12 = (bf16[384,512]{1,0:T(8,128)(2,1)S(1)}, bf16[384,512]{1,0:T(8,128)(2,1)S(1)}, u32[]{:S(2)}, u32[]{:S(2)}) collective-permute-start(bf16[384,512]{1,0:T(8,128)(2,1)S(1)} %get-tuple-element.93), channel_id=1, source_target_pairs={{0,3},{1,0},{2,1},{3,2},{4,7},{5,4},{6,5},{7,6},{8,11},{9,8},{10,9... | collective-permute-start | bytes 1179656 | tf_op jit(solution)/shard_map/ppermute | solution.py:26
  66.5 12.8 %collective-permute-start.15 = (bf16[384,512]{1,0:T(8,128)(2,1)S(1)}, bf16[384,512]{1,0:T(8,128)(2,1)S(1)}, u32[]{:S(2)}, u32[]{:S(2)}) collective-permute-start(bf16[384,512]{1,0:T(8,128)(2,1)S(1)} %get-tuple-element.96), channel_id=1, source_target_pairs={{0,1},{1,2},{2,3},{3,0},{4,5},{5,6},{6,7},{7,4},{8,9},{9,10},{10,1... | collective-permute-start | bytes 1179656 | tf_op jit(solution)/shard_map/ppermute | solution.py:26
  69.6 16.7 %collective-permute-start.17 = (bf16[384,512]{1,0:T(8,128)(2,1)S(1)}, bf16[384,512]{1,0:T(8,128)(2,1)S(1)}, u32[]{:S(2)}, u32[]{:S(2)}) collective-permute-start(bf16[384,512]{1,0:T(8,128)(2,1)S(1)} %shard_map.182), channel_id=1, source_target_pairs={{0,3},{1,0},{2,1},{3,2},{4,7},{5,4},{6,5},{7,6},{8,11},{9,8},{10,9... | collective-permute-start | bytes 1179656 | tf_op jit(solution)/shard_map/ppermute | solution.py:26
  71.3 16.4 %collective-permute-start.14 = (bf16[384,512]{1,0:T(8,128)(2,1)S(1)}, bf16[384,512]{1,0:T(8,128)(2,1)S(1)}, u32[]{:S(2)}, u32[]{:S(2)}) collective-permute-start(bf16[384,512]{1,0:T(8,128)(2,1)S(1)} %shard_map.181), channel_id=1, source_target_pairs={{0,1},{1,2},{2,3},{3,0},{4,5},{5,6},{6,7},{7,4},{8,9},{9,10},{10,1... | collective-permute-start | bytes 1179656 | tf_op jit(solution)/shard_map/ppermute | solution.py:26
  89.0 37.1 %all-to-all-start.1 = ((bf16[64,48,128]{2,1,0:T(8,128)(2,1)}), bf16[64,48,128]{2,1,0:T(8,128)(2,1)S(1)}, u32[]{:S(2)}, u32[]{:S(2)}) async-start(bf16[64,48,128]{2,1,0:T(8,128)(2,1)} %bitcast.9), calls=%async_computation.1 | async-start | bytes 1572864 | tf_op jit(solution)/shard_map/all_to_all | solution.py:541
  126.6 7.2 %collective-permute-start.18 = (bf16[256,512]{1,0:T(8,128)(2,1)S(1)}, bf16[256,512]{1,0:T(8,128)(2,1)S(1)}, u32[]{:S(2)}, u32[]{:S(2)}) collective-permute-start(bf16[256,512]{1,0:T(8,128)(2,1)S(1)} %shard_map.185.own.refs_0_), channel_id=1, source_target_pairs={{0,3},{1,0},{2,1},{3,2},{4,7},{5,4},{6,5},{7,6},{8,11},{9,8},{10,9... | collective-permute-start | bytes 786440 | tf_op jit(solution)/shard_map/ppermute | solution.py:26
  127.2 8.1 %collective-permute-start.19 = (bf16[256,512]{1,0:T(8,128)(2,1)S(1)}, bf16[256,512]{1,0:T(8,128)(2,1)S(1)}, u32[]{:S(2)}, u32[]{:S(2)}) collective-permute-start(bf16[256,512]{1,0:T(8,128)(2,1)S(1)} %shard_map.185.own.refs_0_), channel_id=1, source_target_pairs={{0,1},{1,2},{2,3},{3,0},{4,5},{5,6},{6,7},{7,4},{8,9},{9,10},{10,1... | collective-permute-start | bytes 786440 | tf_op jit(solution)/shard_map/ppermute | solution.py:26
  137.1 14.3 %collective-permute-start.28 = (bf16[256,1536]{1,0:T(8,128)(2,1)}, bf16[256,1536]{1,0:T(8,128)(2,1)S(1)}, u32[]{:S(2)}, u32[]{:S(2)}) collective-permute-start(bf16[256,1536]{1,0:T(8,128)(2,1)} %get-tuple-element.121), channel_id=1, source_target_pairs={{0,4},{4,0},{1,5},{5,1},{2,6},{6,2},{3,7},{7,3},{8,12},{12,8},{9,1... | collective-permute-start | bytes 2359304 | tf_op jit(solution)/shard_map/ppermute | solution.py:26
  138.9 9.4 %collective-permute-start.20 = (bf16[256,512]{1,0:T(8,128)(2,1)S(1)}, bf16[256,512]{1,0:T(8,128)(2,1)S(1)}, u32[]{:S(2)}, u32[]{:S(2)}) collective-permute-start(bf16[256,512]{1,0:T(8,128)(2,1)S(1)} %shard_map.185.own.refs_0_), channel_id=1, source_target_pairs={{0,2},{1,3},{2,0},{3,1},{4,6},{5,7},{6,4},{7,5},{8,10},{9,11},{10,... | collective-permute-start | bytes 786440 | tf_op jit(solution)/shard_map/ppermute | solution.py:26
  152.8 9.1 %collective-permute-start.30 = (bf16[64,2048]{1,0:T(8,128)(2,1)S(1)}, bf16[64,2048]{1,0:T(8,128)(2,1)S(1)}, u32[]{:S(2)}, u32[]{:S(2)}) collective-permute-start(bf16[64,2048]{1,0:T(8,128)(2,1)S(1)} %get-tuple-element.125), channel_id=1, source_target_pairs={{0,16},{8,24},{16,0},{24,8},{1,17},{9,25},{17,1},{25,9},{2,18},{10... | collective-permute-start | bytes 786440 | tf_op jit(solution)/shard_map/ppermute | solution.py:26
  154.5 45.9 %collective-permute-start.26 = (bf16[768,512]{1,0:T(8,128)(2,1)}, bf16[768,512]{1,0:T(8,128)(2,1)}, u32[]{:S(2)}, u32[]{:S(2)}) collective-permute-start(bf16[768,512]{1,0:T(8,128)(2,1)} %get-tuple-element.117.refs_0_), channel_id=1, source_target_pairs={{0,3},{1,0},{2,1},{3,2},{4,7},{5,4},{6,5},{7,6},{8,11},{9,8},{10,9... | collective-permute-start | bytes 2359304 | tf_op jit(solution)/shard_map/ppermute | solution.py:26
  154.5 45.9 %collective-permute-start.27 = (bf16[768,512]{1,0:T(8,128)(2,1)}, bf16[768,512]{1,0:T(8,128)(2,1)}, u32[]{:S(2)}, u32[]{:S(2)}) collective-permute-start(bf16[768,512]{1,0:T(8,128)(2,1)} %get-tuple-element.117.refs_0_), channel_id=1, source_target_pairs={{0,1},{1,2},{2,3},{3,0},{4,5},{5,6},{6,7},{7,4},{8,9},{9,10},{10,1... | collective-permute-start | bytes 2359304 | tf_op jit(solution)/shard_map/ppermute | solution.py:26
  156.0 47.9 %collective-permute-start.25 = (bf16[768,512]{1,0:T(8,128)(2,1)}, bf16[768,512]{1,0:T(8,128)(2,1)S(1)}, u32[]{:S(2)}, u32[]{:S(2)}) collective-permute-start(bf16[768,512]{1,0:T(8,128)(2,1)} %get-tuple-element.117.refs_0_), channel_id=1, source_target_pairs={{0,2},{1,3},{2,0},{3,1},{4,6},{5,7},{6,4},{7,5},{8,10},{9,11},{10,... | collective-permute-start | bytes 2359304 | tf_op jit(solution)/shard_map/ppermute | solution.py:26
  156.1 12.2 %collective-permute-start.31 = (bf16[64,2048]{1,0:T(8,128)(2,1)S(1)}, bf16[64,2048]{1,0:T(8,128)(2,1)S(1)}, u32[]{:S(2)}, u32[]{:S(2)}) collective-permute-start(bf16[64,2048]{1,0:T(8,128)(2,1)S(1)} %get-tuple-element.126), channel_id=1, source_target_pairs={{0,8},{8,16},{16,24},{24,0},{1,9},{9,17},{17,25},{25,1},{2,10},{10... | collective-permute-start | bytes 786440 | tf_op jit(solution)/shard_map/ppermute | solution.py:26
  161.9 6.4 %collective-permute-start.32 = (bf16[64,2048]{1,0:T(8,128)(2,1)S(1)}, bf16[64,2048]{1,0:T(8,128)(2,1)S(1)}, u32[]{:S(2)}, u32[]{:S(2)}) collective-permute-start(bf16[64,2048]{1,0:T(8,128)(2,1)S(1)} %get-tuple-element.127), channel_id=1, source_target_pairs={{0,24},{8,0},{16,8},{24,16},{1,25},{9,1},{17,9},{25,17},{2,26},{10... | collective-permute-start | bytes 786440 | tf_op jit(solution)/shard_map/ppermute | solution.py:26
  169.1 41.5 %all-to-all-start.2 = ((bf16[8,8,2048]{2,1,0:T(8,128)(2,1)}), bf16[8,8,2048]{2,1,0:T(8,128)(2,1)S(1)}, u32[]{:S(2)}, u32[]{:S(2)}) async-start(bf16[8,8,2048]{2,1,0:T(8,128)(2,1)} %bitcast.17), calls=%async_computation.2 | async-start | bytes 524288 | tf_op jit(solution)/shard_map/all_to_all | solution.py:604
  175.7 16.0 %collective-permute-start.21 = (f32[8,256]{1,0:T(8,128)S(1)}, f32[8,256]{1,0:T(8,128)S(1)}, u32[]{:S(2)}, u32[]{:S(2)}) collective-permute-start(f32[8,256]{1,0:T(8,128)S(1)} %get-tuple-element.111.own), channel_id=1, source_target_pairs={{0,1},{1,2},{2,3},{3,0},{4,5},{5,6},{6,7},{7,4},{8,9},{9,10},{10,1... | collective-permute-start | bytes 24584 | tf_op jit(solution)/shard_map/ppermute | solution.py:26
  175.7 16.0 %collective-permute-start.22 = (f32[8,256]{1,0:T(8,128)S(1)}, f32[8,256]{1,0:T(8,128)S(1)}, u32[]{:S(2)}, u32[]{:S(2)}) collective-permute-start(f32[8,256]{1,0:T(8,128)S(1)} %get-tuple-element.111.own), channel_id=1, source_target_pairs={{0,3},{1,0},{2,1},{3,2},{4,7},{5,4},{6,5},{7,6},{8,11},{9,8},{10,9... | collective-permute-start | bytes 24584 | tf_op jit(solution)/shard_map/ppermute | solution.py:26
  196.0 11.1 %collective-permute-start.24 = (f32[32,512]{1,0:T(8,128)S(1)}, f32[32,512]{1,0:T(8,128)S(1)}, u32[]{:S(2)}, u32[]{:S(2)}) collective-permute-start(f32[32,512]{1,0:T(8,128)S(1)} %get-tuple-element.114), channel_id=1, source_target_pairs={{4,0},{8,4},{12,8},{16,12},{20,16},{24,20},{28,24},{32,28},{36,32}... | collective-permute-start | bytes 196616 | tf_op jit(solution)/shard_map/ppermute | solution.py:32
  (25 other events, 348.0 us)
